TPU v7x, 256 devices: a whole 4x4x8 slice. The times are simulated.
256 devices in a mesh: ep: 16 (over y, x), tp: 16 (over z, core).
Axes of the slice: x: 4, y: 4, z: 8, core: 2. Of those that a mesh axis runs over, the one named last changes fastest.
Arguments:
- tokens: bfloat16 [256, 2048], P('ep'), may hold values from -6 to 6
- norm_gain: float32 [2048], replicated, may hold values from 0.1 to 1.9
- w_query: bfloat16 [2048, 2048], P(None, 'tp'), may hold values from -0.125 to 0.125
- w_key: bfloat16 [2048, 2048], P(None, 'tp'), may hold values from -0.125 to 0.125
- w_value: bfloat16 [2048, 2048], P(None, 'tp'), may hold values from -0.125 to 0.125
- query_gain: float32 [128], replicated, may hold values from 0.1 to 1.9
- key_gain: float32 [128], replicated, may hold values from 0.1 to 1.9
- score_bias: float32 [16], P('tp'), may hold values from -11 to -3.5
- key_cache: bfloat16 [256, 1024, 2048], P('ep', None, 'tp'), may hold values from -6 to 6
- value_cache: bfloat16 [256, 1024, 2048], P('ep', None, 'tp'), may hold values from -6 to 6
- lengths: int32 [256], P('ep'), may hold values from 128 to 1024
- w_out: bfloat16 [2048, 2048], P('tp'), may hold values from -0.125 to 0.125
- post_gain: float32 [2048], replicated, may hold values from 0.1 to 1.9
- routes: int32 [256, 6], P('ep'), may hold values from 0 to 63, all different within a row; in each aligned block of 16 rows (0 to 15, 16 to 31, ...) at most 3 rows name the same one
- route_weight: float32 [256, 6], P('ep'), may hold values from 0.25 to 2
- expert_gate: bfloat16 [256, 2048, 128], P(('ep', 'tp')), may hold values from -0.125 to 0.125
- expert_up: bfloat16 [256, 2048, 128], P(('ep', 'tp')), may hold values from -0.125 to 0.125
- expert_down: bfloat16 [256, 128, 2048], P(('ep', 'tp')), may hold values from -0.25 to 0.25
- shared_gate: bfloat16 [2048, 512], P(None, 'tp'), may hold values from -0.125 to 0.125
- shared_up: bfloat16 [2048, 512], P(None, 'tp'), may hold values from -0.125 to 0.125
- shared_down: bfloat16 [512, 2048], P('tp'), may hold values from -0.25 to 0.25
Outputs:
- mixed: bfloat16 [256, 2048], P('ep', 'tp')
- new_keys: bfloat16 [256, 2048], P('ep', 'tp')
- new_values: bfloat16 [256, 2048], P('ep', 'tp')
Inputs may be any that keep to these rules, and one draw needn't show every extreme that they name: `routes`: within the rows of one device no expert is named by more than 3 rows, a bound that some block reaches of them.
All inputs are finite; a program needn't handle non-finite values.
Results may differ from a plain program's by a relative error of at most 0.008.
Values may be sent and summed in bfloat16 or wider, within the bound.
No kernel may reach another device: no remote copies, remote signals or barrier semaphores. Data moves between devices by JAX's collectives and lax.ppermute only.
A program may use at most 64 MiB of HBM per device.

v0:
```python
import jax
import jax.numpy as jnp
from jax import lax
from jax.sharding import PartitionSpec as P

EPS = 1e-06


def rows_for(lines, devices):
    spare = -lines.shape[0] % devices
    if not spare:
        return lines
    return jnp.concatenate([lines, jnp.zeros((spare, *lines.shape[1:]), lines.dtype)])


def in_order(pieces, dim):
    dims = list(pieces.shape[1:])
    dims[dim] *= pieces.shape[0]
    return jnp.moveaxis(pieces, 0, dim).reshape(dims)


def sent_to_all(x, axis):
    copies = jnp.broadcast_to(x, (lax.axis_size(axis), *x.shape))
    return lax.all_to_all(copies, axis, split_axis=0, concat_axis=0, tiled=True)


def gathered_copies(x, axis, dim):
    return in_order(sent_to_all(x, axis), dim)


def cut_along(x, dim, devices):
    before, after = (x.shape[:dim], x.shape[dim + 1 :])
    return jnp.moveaxis(x.reshape(*before, devices, -1, *after), dim, 0)


def sent_and_summed(x, axis, dim):
    pieces = cut_along(x, dim, lax.axis_size(axis))
    arrived = lax.all_to_all(pieces, axis, split_axis=0, concat_axis=0, tiled=True)
    return arrived.sum(axis=0)


def sum_by_parts(x, axes):
    lines = x.reshape(-1, x.shape[-1])
    padded = rows_for(lines, lax.axis_size(axes))
    whole = gathered_copies(sent_and_summed(padded, axes, 0), axes, 0)
    return lax.slice_in_dim(whole, 0, len(lines)).reshape(x.shape)


def rms_scale(values, gain_vec):
    mean_sq = jnp.mean(values * values, axis=-1, keepdims=True)
    return values * lax.rsqrt(mean_sq + EPS) * gain_vec


def slot_table(route_rows, first_expert, expert_count, capacity):
    flattened = route_rows.reshape(-1)
    relative = flattened - first_expert
    expert_ids = jnp.arange(expert_count, dtype=jnp.int32)
    member = (relative[:, None] == expert_ids[None, :]).astype(jnp.int32)
    ranking = jnp.cumsum(member, axis=0) - member
    slot_index = jnp.sum(ranking * member, axis=1)
    inside = jnp.sum(member, axis=1) > 0
    target = relative * capacity + slot_index
    columns = jnp.arange(expert_count * capacity, dtype=jnp.int32)
    return ((target[:, None] == columns[None, :]) & inside[:, None]).astype(jnp.float32)


def row_owner(row_count, topk):
    assigned = jnp.arange(row_count * topk, dtype=jnp.int32) // topk
    return (assigned[:, None] == jnp.arange(row_count, dtype=jnp.int32)[None, :]).astype(
        jnp.float32
    )


def local(
    tokens,
    norm_gain,
    w_query,
    w_key,
    w_value,
    query_gain,
    key_gain,
    score_bias,
    key_cache,
    value_cache,
    lengths,
    w_out,
    post_gain,
    routes,
    route_weight,
    expert_gate,
    expert_up,
    expert_down,
    shared_gate,
    shared_up,
    shared_down,
):
    seq_rows, width = tokens.shape
    head_count = score_bias.shape[0]
    head_size = query_gain.shape[0]
    cache_len = key_cache.shape[1]
    topk = routes.shape[1]
    group_count = lax.axis_size("ep")
    per_group = lax.axis_size("tp") // 4
    experts = group_count * per_group
    capacity = min(seq_rows, max(2, 2 * seq_rows * topk // experts))
    local_part = lax.axis_index("tp") // 4
    normed = rms_scale(tokens.astype(jnp.float32), norm_gain).astype(jnp.bfloat16)
    queries = jnp.dot(normed, w_query, preferred_element_type=jnp.float32).reshape(
        seq_rows, head_count, head_size
    )
    queries = rms_scale(queries, query_gain).astype(jnp.bfloat16)
    key_proj = jnp.dot(normed, w_key, preferred_element_type=jnp.float32).reshape(
        seq_rows, head_count, head_size
    )
    new_keys = (
        rms_scale(key_proj, key_gain).astype(jnp.bfloat16).reshape(seq_rows, head_count * head_size)
    )
    new_values = jnp.dot(normed, w_value, preferred_element_type=jnp.float32).astype(jnp.bfloat16)
    key_blocks = key_cache.reshape(seq_rows, cache_len, head_count, head_size)
    value_blocks = value_cache.reshape(seq_rows, cache_len, head_count, head_size)
    logits = jnp.einsum("shd,slhd->shl", queries, key_blocks, preferred_element_type=jnp.float32)
    logits = logits * head_size ** (-0.5) + score_bias[None, :, None]
    positions = jnp.arange(cache_len, dtype=jnp.int32)
    visible = (positions[None, :] < lengths[:, None])[:, None, :]
    log_beta = jax.nn.log_sigmoid(logits)
    log_keep = jnp.where(visible, jax.nn.log_sigmoid(-logits), 0.0)
    later_sum = lax.cumsum(log_keep, axis=2, reverse=True) - log_keep
    weights = jnp.where(visible, jnp.exp(log_beta + later_sum), 0.0).astype(jnp.bfloat16)
    attended = jnp.einsum(
        "shl,slhd->shd", weights, value_blocks, preferred_element_type=jnp.float32
    )
    attended = attended.astype(jnp.bfloat16).reshape(seq_rows, head_count * head_size)
    attn_part = jnp.dot(attended, w_out, preferred_element_type=jnp.float32)
    attn = sum_by_parts(attn_part, "tp")
    hstate = (tokens.astype(jnp.float32) + attn).astype(jnp.bfloat16)
    h_normed = rms_scale(hstate.astype(jnp.float32), post_gain).astype(jnp.bfloat16)
    owners = row_owner(seq_rows, topk)
    full_table = slot_table(routes, 0, experts, capacity)
    full_table = full_table.reshape(seq_rows * topk, group_count, per_group, capacity)
    own_table = lax.dynamic_index_in_dim(full_table, local_part, 2, keepdims=False)
    own_table = own_table.reshape(seq_rows * topk, group_count * capacity)
    picker = jnp.dot(own_table.T, owners, precision=lax.Precision.HIGHEST).astype(jnp.bfloat16)
    outgoing = jnp.dot(picker, h_normed, preferred_element_type=jnp.float32).astype(jnp.bfloat16)
    outgoing = outgoing.reshape(group_count, capacity, width)
    received = lax.all_to_all(outgoing, "ep", split_axis=0, concat_axis=0, tiled=True)
    gate_pre = jnp.einsum(
        "gcd,df->gcf", received, expert_gate[0], preferred_element_type=jnp.float32
    )
    up_pre = jnp.einsum("gcd,df->gcf", received, expert_up[0], preferred_element_type=jnp.float32)
    hidden = (jax.nn.silu(gate_pre) * up_pre).astype(jnp.bfloat16)
    expert_partial = jnp.einsum(
        "gcf,fd->gcd", hidden, expert_down[0], preferred_element_type=jnp.float32
    )
    returned = lax.all_to_all(expert_partial, "ep", split_axis=0, concat_axis=0, tiled=True)
    returned = returned.reshape(group_count * capacity, width)
    weighted = own_table * route_weight.reshape(-1)[:, None]
    combiner = jnp.dot(owners.T, weighted, precision=lax.Precision.HIGHEST)
    routed_part = jnp.dot(combiner, returned, precision=lax.Precision.HIGHEST)
    shared_hidden = (
        jax.nn.silu(jnp.dot(h_normed, shared_gate, preferred_element_type=jnp.float32))
        * jnp.dot(h_normed, shared_up, preferred_element_type=jnp.float32)
    ).astype(jnp.bfloat16)
    shared_partial = jnp.dot(shared_hidden, shared_down, preferred_element_type=jnp.float32)
    branch_sum = sent_and_summed(routed_part + shared_partial, "tp", 1)
    slice_width = branch_sum.shape[1]
    offset = lax.axis_index("tp") * slice_width
    own_slice = lax.dynamic_slice_in_dim(hstate, offset, slice_width, 1).astype(jnp.float32)
    mixed = (own_slice + branch_sum).astype(jnp.bfloat16)
    return (mixed, new_keys, new_values)


def solution(mesh):
    placed = (
        P("ep", None),
        P(),
        P(None, "tp"),
        P(None, "tp"),
        P(None, "tp"),
        P(),
        P(),
        P("tp"),
        P("ep", None, "tp"),
        P("ep", None, "tp"),
        P("ep"),
        P("tp", None),
        P(),
        P("ep", None),
        P("ep", None),
        P(("ep", "tp"), None, None),
        P(("ep", "tp"), None, None),
        P(("ep", "tp"), None, None),
        P(None, "tp"),
        P(None, "tp"),
        P("tp", None),
    )
    return jax.shard_map(
        local,
        mesh=mesh,
        in_specs=placed,
        out_specs=(P("ep", "tp"), P("ep", "tp"), P("ep", "tp")),
        check_vma=False,
    )
```

profile of v0, /device:TPU:1, one launch (start us, length us, event | category | flops | bytes accessed | tf_op | source)
XLA Modules:
  0.0 113.5 jit_solution(10183975606482362335)
XLA Ops:
  0.7 1.0 fusion.15
  1.7 1.4 %multiply_reduce_fusion.1 = (f32[16]{0:T(128)S(1)}, f32[16,128]{1,0:T(8,128)S(1)}) fusion(bf16[2048,128]{1,0:T(8,128)(2,1)} %param.23, bf16[16,2048]{1,0:T(8,128)(2,1)} %param.21, f32[2048]{0:T(1024)} %param.22, f32[16]{0:T(128)S(1)} %add_rsqrt_fusion.3), kind=kOutput, calls=%fused_computation.78 | convolution fusion | flops 8523760 | bytes 606336 | tf_op jit(solution)/shard_map/dot_general | solution.py:108
  3.8 0.7 fusion.54
  4.6 3.4 %fusion.47 = f32[16,1,1024]{2,1,0:T(1,128)S(1)} fusion(bf16[16,1024,128]{2,1,0:T(8,128)(2,1)} %param.29, bf16[16,128,1]{1,0,2:T(8,128)(2,1)S(1)} %fusion.54), kind=kOutput, calls=%fused_computation.67 | convolution fusion | flops 4194304 | bytes 4263936 | tf_op jit(solution)/shard_map/shd,slhd->shl/dot_general | solution.py:121
  8.1 19.8 %reduce-window.6 = f32[16,1,8,128]{3,2,1,0:T(8,128)S(1)} reduce-window(f32[16,1,8,128]{3,2,1,0:T(8,128)S(1)} %bitcast.88, f32[]{:T(128)} %constant.58.clone.1), window={size=1x1x1x128 pad=0_0x0_0x0_0x0_127}, to_apply=%region_2.3 | reduce-window | flops 2080768 | bytes 131076 | tf_op jit(solution)/shard_map/reduce-window
  28.4 2.9 %fusion.28 = f32[16,1,128]{2,1,0:T(1,128)S(1)} fusion(bf16[16,1024,128]{2,1,0:T(8,128)(2,1)} %param.30, bf16[16,1024,1]{1,0,2:T(8,128)(2,1)S(1)} %fusion.34), kind=kOutput, calls=%fused_computation.44 | convolution fusion | flops 4194304 | bytes 4235264 | tf_op jit(solution)/shard_map/shl,slhd->shd/dot_general | solution.py:129
  31.6 0.8 copy.37
  32.3 10.0 %all-to-all-start = ((f32[16,1,2048]{2,1,0:T(1,128)}), f32[16,1,2048]{2,1,0:T(1,128)S(1)}, u32[]{:S(2)}, u32[]{:S(2)}) async-start(f32[16,1,2048]{2,1,0:T(1,128)} %copy.37), calls=%async_computation | async-start | bytes 262144 | tf_op jit(solution)/shard_map/all_to_all | solution.py:38
  43.2 8.0 %all-to-all-done = f32[16,1,2048]{2,1,0:T(1,128)S(1)} async-done(((f32[16,1,2048]{2,1,0:T(1,128)}), f32[16,1,2048]{2,1,0:T(1,128)S(1)}, u32[]{:S(2)}, u32[]{:S(2)}) %all-to-all-start) | async-done | bytes 131104 | tf_op jit(solution)/shard_map/all_to_all | solution.py:38
  51.3 0.7 broadcast_in_dim.4
  52.0 3.4 %all-to-all-start.1 = ((f32[16,1,2048]{2,1,0:T(1,128)}), f32[16,1,2048]{2,1,0:T(1,128)S(1)}, u32[]{:S(2)}, u32[]{:S(2)}) async-start(f32[16,1,2048]{2,1,0:T(1,128)} %broadcast_in_dim.4), calls=%async_computation.1 | async-start | bytes 262144 | tf_op jit(solution)/shard_map/all_to_all | solution.py:24
  56.3 8.1 %all-to-all-done.1 = f32[16,1,2048]{2,1,0:T(1,128)S(1)} async-done(((f32[16,1,2048]{2,1,0:T(1,128)}), f32[16,1,2048]{2,1,0:T(1,128)S(1)}, u32[]{:S(2)}, u32[]{:S(2)}) %all-to-all-start.1) | async-done | bytes 131104 | tf_op jit(solution)/shard_map/all_to_all | solution.py:24
  64.8 0.8 reshape.235
  65.6 6.8 %all-to-all-start.2 = ((bf16[16,3,2048]{2,1,0:T(4,128)(2,1)}), bf16[16,3,2048]{2,1,0:T(4,128)(2,1)S(1)}, u32[]{:S(2)}, u32[]{:S(2)}) async-start(bf16[16,3,2048]{2,1,0:T(4,128)(2,1)} %reshape.235), calls=%async_computation.2 | async-start | bytes 524288 | tf_op jit(solution)/shard_map/all_to_all | solution.py:145
  72.6 8.3 %all-to-all-done.2 = bf16[16,3,2048]{2,1,0:T(4,128)(2,1)S(1)} async-done(((bf16[16,3,2048]{2,1,0:T(4,128)(2,1)}), bf16[16,3,2048]{2,1,0:T(4,128)(2,1)S(1)}, u32[]{:S(2)}, u32[]{:S(2)}) %all-to-all-start.2) | async-done | bytes 196640 | tf_op jit(solution)/shard_map/all_to_all | solution.py:145
  81.7 1.1 copy.42
  82.8 3.6 %all-to-all-start.3 = ((f32[16,3,2048]{2,1,0:T(4,128)}), f32[16,3,2048]{2,1,0:T(4,128)S(1)}, u32[]{:S(2)}, u32[]{:S(2)}) async-start(f32[16,3,2048]{2,1,0:T(4,128)} %copy.42), calls=%async_computation.3 | async-start | bytes 1048576 | tf_op jit(solution)/shard_map/all_to_all | solution.py:154
  86.6 10.3 %all-to-all-done.3 = f32[16,3,2048]{2,1,0:T(4,128)S(1)} async-done(((f32[16,3,2048]{2,1,0:T(4,128)}), f32[16,3,2048]{2,1,0:T(4,128)S(1)}, u32[]{:S(2)}, u32[]{:S(2)}) %all-to-all-start.3) | async-done | bytes 393248 | tf_op jit(solution)/shard_map/all_to_all | solution.py:154
  97.9 0.6 copy.78
  98.5 5.2 %all-to-all-start.4 = ((f32[16,16,128]{2,1,0:T(8,128)}), f32[16,16,128]{2,1,0:T(8,128)S(1)}, u32[]{:S(2)}, u32[]{:S(2)}) async-start(f32[16,16,128]{2,1,0:T(8,128)} %bitcast.81), calls=%async_computation.4 | async-start | bytes 262144 | tf_op jit(solution)/shard_map/all_to_all | solution.py:38
  103.7 0.7 multiply_convert_fusion
  104.4 0.8 convolution_convert_fusion.2
  105.2 7.7 %all-to-all-done.4 = f32[16,16,128]{2,1,0:T(8,128)S(1)} async-done(((f32[16,16,128]{2,1,0:T(8,128)}), f32[16,16,128]{2,1,0:T(8,128)S(1)}, u32[]{:S(2)}, u32[]{:S(2)}) %all-to-all-start.4) | async-done | bytes 131104 | tf_op jit(solution)/shard_map/all_to_all | solution.py:38
  112.9 0.6 add_convert_fusion
  (73 shorter events, 5.0 us)
Async XLA Ops:
  0.6 80.6 %copy-start = (bf16[1,128,2048]{2,1,0:T(8,128)(2,1)S(1)}, bf16[1,128,2048]{2,1,0:T(8,128)(2,1)}, u32[]{:S(2)}) copy-start(bf16[1,128,2048]{2,1,0:T(8,128)(2,1)} %param.38) | copy-start | bytes 1572868
  0.6 7.4 %copy-start.13 = (s32[16]{0:T(128)S(1)}, s32[16]{0:T(128)}, u32[]{:S(2)}) copy-start(s32[16]{0:T(128)} %param.31) | copy-start | bytes 196
  4.6 26.8 %copy-start.4 = (bf16[128,2048]{1,0:T(8,128)(2,1)S(1)}, bf16[128,2048]{1,0:T(8,128)(2,1)}, u32[]{:S(2)}) copy-start(bf16[128,2048]{1,0:T(8,128)(2,1)} %param.32) | copy-start | bytes 1572868
  8.0 34.3 %copy-start.11 = (s32[16,6]{0,1:T(8,128)S(1)}, s32[16,6]{0,1:T(8,128)}, u32[]{:S(2)}) copy-start(s32[16,6]{0,1:T(8,128)} %param.34) | copy-start | bytes 1156
  8.0 47.7 %copy-start.12 = (f32[16,6]{0,1:T(8,128)S(1)}, f32[16,6]{0,1:T(8,128)}, u32[]{:S(2)}) copy-start(f32[16,6]{0,1:T(8,128)} %param.35) | copy-start | bytes 1156
  8.0 47.9 %copy-start.1 = (bf16[16,2048]{1,0:T(8,128)(2,1)S(1)}, bf16[16,2048]{1,0:T(8,128)(2,1)}, u32[]{:S(2)}) copy-start(bf16[16,2048]{1,0:T(8,128)(2,1)} %param.21) | copy-start | bytes 196612
  8.0 47.9 %copy-start.3 = (bf16[2048,128]{1,0:T(8,128)(2,1)S(1)}, bf16[2048,128]{1,0:T(8,128)(2,1)}, u32[]{:S(2)}) copy-start(bf16[2048,128]{1,0:T(8,128)(2,1)} %param.24) | copy-start | bytes 1572868
  8.0 47.9 %copy-start.9 = (f32[2048]{0:T(1024)S(1)}, f32[2048]{0:T(1024)}, u32[]{:S(2)}) copy-start(f32[2048]{0:T(1024)} %param.22) | copy-start | bytes 24580
  8.0 56.5 %copy-start.10 = (f32[2048]{0:T(1024)S(1)}, f32[2048]{0:T(1024)}, u32[]{:S(2)}) copy-start(f32[2048]{0:T(1024)} %param.33) | copy-start | bytes 24580
  28.4 52.5 %copy-start.5 = (bf16[1,2048,128]{2,1,0:T(8,128)(2,1)S(1)}, bf16[1,2048,128]{2,1,0:T(8,128)(2,1)}, u32[]{:S(2)}) copy-start(bf16[1,2048,128]{2,1,0:T(8,128)(2,1)} %param.36) | copy-start | bytes 1572868
  28.4 52.8 %copy-start.2 = (bf16[1,2048,128]{2,1,0:T(8,128)(2,1)S(1)}, bf16[1,2048,128]{2,1,0:T(8,128)(2,1)}, u32[]{:S(2)}) copy-start(bf16[1,2048,128]{2,1,0:T(8,128)(2,1)} %param.37) | copy-start | bytes 1572868
  31.6 54.8 %copy-start.15 = (bf16[2048,32]{0,1:T(8,128)(2,1)S(1)}, bf16[2048,32]{0,1:T(8,128)(2,1)}, u32[]{:S(2)}) copy-start(bf16[2048,32]{0,1:T(8,128)(2,1)} %param.39) | copy-start | bytes 393220
  32.3 18.9 %all-to-all-start = ((f32[16,1,2048]{2,1,0:T(1,128)}), f32[16,1,2048]{2,1,0:T(1,128)S(1)}, u32[]{:S(2)}, u32[]{:S(2)}) async-start(f32[16,1,2048]{2,1,0:T(1,128)} %copy.37), calls=%async_computation | async-start | bytes 262144 | tf_op jit(solution)/shard_map/all_to_all | solution.py:38
  52.0 12.3 %all-to-all-start.1 = ((f32[16,1,2048]{2,1,0:T(1,128)}), f32[16,1,2048]{2,1,0:T(1,128)S(1)}, u32[]{:S(2)}, u32[]{:S(2)}) async-start(f32[16,1,2048]{2,1,0:T(1,128)} %broadcast_in_dim.4), calls=%async_computation.1 | async-start | bytes 262144 | tf_op jit(solution)/shard_map/all_to_all | solution.py:24
  55.4 42.0 %copy-start.7 = (bf16[32,2048]{1,0:T(8,128)(2,1)S(1)}, bf16[32,2048]{1,0:T(8,128)(2,1)}, u32[]{:S(2)}) copy-start(bf16[32,2048]{1,0:T(8,128)(2,1)} %param.41) | copy-start | bytes 393220
  55.4 42.0 %copy-start.8 = (bf16[2048,32]{0,1:T(8,128)(2,1)S(1)}, bf16[2048,32]{0,1:T(8,128)(2,1)}, u32[]{:S(2)}) copy-start(bf16[2048,32]{0,1:T(8,128)(2,1)} %param.40) | copy-start | bytes 393220
  64.5 39.2 %copy-start.14 = (f32[128]{0:T(128)S(1)}, f32[128]{0:T(128)}, u32[]{:S(2)}) copy-start(f32[128]{0:T(128)} %param.27) | copy-start | bytes 1540
  64.8 39.6 %copy-start.6 = (bf16[2048,128]{1,0:T(8,128)(2,1)S(1)}, bf16[2048,128]{1,0:T(8,128)(2,1)}, u32[]{:S(2)}) copy-start(bf16[2048,128]{1,0:T(8,128)(2,1)} %param.25) | copy-start | bytes 1572868
  65.6 15.3 %all-to-all-start.2 = ((bf16[16,3,2048]{2,1,0:T(4,128)(2,1)}), bf16[16,3,2048]{2,1,0:T(4,128)(2,1)S(1)}, u32[]{:S(2)}, u32[]{:S(2)}) async-start(bf16[16,3,2048]{2,1,0:T(4,128)(2,1)} %reshape.235), calls=%async_computation.2 | async-start | bytes 524288 | tf_op jit(solution)/shard_map/all_to_all | solution.py:145
  82.8 14.1 %all-to-all-start.3 = ((f32[16,3,2048]{2,1,0:T(4,128)}), f32[16,3,2048]{2,1,0:T(4,128)S(1)}, u32[]{:S(2)}, u32[]{:S(2)}) async-start(f32[16,3,2048]{2,1,0:T(4,128)} %copy.42), calls=%async_computation.3 | async-start | bytes 1048576 | tf_op jit(solution)/shard_map/all_to_all | solution.py:154
  98.5 14.4 %all-to-all-start.4 = ((f32[16,16,128]{2,1,0:T(8,128)}), f32[16,16,128]{2,1,0:T(8,128)S(1)}, u32[]{:S(2)}, u32[]{:S(2)}) async-start(f32[16,16,128]{2,1,0:T(8,128)} %bitcast.81), calls=%async_computation.4 | async-start | bytes 262144 | tf_op jit(solution)/shard_map/all_to_all | solution.py:38
where the time goes:
time: 114 us
  waiting for transfers between devices  42.4 us (37%)
  starting transfers between devices  28.9 us (25%)
  other arithmetic  24 us (21%)
  matrix products  11.6 us (10%)
  local copies, waits for them, and re-layouts  5 us (4%)
  between operations  1.68 us (1%)
    another operation x2, other arithmetic  19.8 us
    all_to_all x2, waiting for transfers between devices, sent_and_summed(): lax.all_to_all(pieces, axis, split_axis=0, concat_axis=0, tiled=True)  15.7 us
    all_to_all x2, starting transfers between devices, sent_and_summed(): lax.all_to_all(pieces, axis, split_axis=0, concat_axis=0, tiled=True)  15.2 us
    all_to_all x1, waiting for transfers between devices, local(): lax.all_to_all(expert_partial, 'ep', split_axis=0, concat_axis=0, tiled=T...  10.3 us
    all_to_all x1, waiting for transfers between devices, local(): lax.all_to_all(outgoing, 'ep', split_axis=0, concat_axis=0, tiled=True)  8.32 us
    all_to_all x1, waiting for transfers between devices, sent_to_all(): return lax.all_to_all(copies, axis, split_axis=0, concat_axis=0, tiled=True)  8.07 us
    all_to_all x1, starting transfers between devices, local(): lax.all_to_all(outgoing, 'ep', split_axis=0, concat_axis=0, tiled=True)  6.76 us
    all_to_all x1, starting transfers between devices, local(): lax.all_to_all(expert_partial, 'ep', split_axis=0, concat_axis=0, tiled=T...  3.57 us
  transfers between devices with their start and end apart: 5, of which 5 were waited for; matrix products, arithmetic and copies ran while one was open for 3% of the time, Pallas kernels for 0%

commit v1 on v0

v1 whole, which is shorter than its diff:
```python
import jax
import jax.numpy as jnp
from jax import lax
from jax.experimental import pallas as pl
from jax.experimental.pallas import tpu as pltpu
from jax.sharding import Mesh, PartitionSpec as P

EPS = 1e-06
BF16 = jnp.bfloat16
F32 = jnp.float32
LANES = 128
EP, TA, TB = 16, 4, 4
ROWS = 16
SLOTS = 4
GROUP = 4
BLOCKS = 16
MIB = 1024 * 1024


def rms_rows(values, gain):
    mean_sq = jnp.mean(values * values, axis=-1, keepdims=True)
    return values * lax.rsqrt(mean_sq + EPS) * gain


def dot(x, w):
    return jnp.dot(x, w, preferred_element_type=F32)


def dot_nt(x, w):
    return lax.dot_general(x, w, (((1,), (1,)), ((), ())), preferred_element_type=F32)


def vmem():
    return pl.BlockSpec(memory_space=pltpu.VMEM)


def smem():
    return pl.BlockSpec(memory_space=pltpu.SMEM)


def hbm():
    return pl.BlockSpec(memory_space=pltpu.HBM)


def route_tables(routes, weights, a, pick_ref, coef_hi_ref, coef_lo_ref):
    experts = EP * TA
    expert_ids = lax.broadcasted_iota(jnp.int32, (experts, ROWS), 0)
    member = jnp.zeros((experts, ROWS), F32)
    weight_of = jnp.zeros((experts, ROWS), F32)
    for k in range(routes.shape[0]):
        hit = routes[k : k + 1, :] == expert_ids
        member = member + jnp.where(hit, 1.0, 0.0)
        weight_of = weight_of + jnp.where(hit, weights[k : k + 1, :], 0.0)
    row_in = lax.broadcasted_iota(jnp.int32, (ROWS, ROWS), 0)
    row_out = lax.broadcasted_iota(jnp.int32, (ROWS, ROWS), 1)
    rank = dot(member.astype(BF16), (row_in < row_out).astype(F32).astype(BF16))
    slot_of = (member * (rank + 1.0)).astype(BF16)

    count = EP * TB * TA * SLOTS
    wide_in = lax.broadcasted_iota(jnp.int32, (ROWS, 64), 0)
    wide_out = lax.broadcasted_iota(jnp.int32, (ROWS, 64), 1)
    widen = (wide_out % ROWS == wide_in).astype(F32).astype(BF16)
    row = lax.broadcasted_iota(jnp.int32, (count, 64), 0)
    lane = lax.broadcasted_iota(jnp.int32, (count, 64), 1)
    owner = (lane == (row // 64) * TA + a).astype(F32).astype(BF16)
    found = dot(owner, dot(slot_of, widen).astype(BF16))
    slot = row % SLOTS
    same_block = (row // SLOTS) % TA == lane // ROWS
    routed = found == (slot + 1).astype(F32)
    shared = lane % ROWS == row // 64
    chosen = jnp.where(slot == SLOTS - 1, shared.astype(F32), routed.astype(F32))
    pick_ref[...] = jnp.where(same_block, chosen, 0.0).astype(BF16)

    turn = (row_in == row_out).astype(F32).astype(BF16)
    spread_row = lax.broadcasted_iota(jnp.int32, (experts, count), 0)
    spread_lane = lax.broadcasted_iota(jnp.int32, (experts, count), 1)
    spread = (spread_row == spread_lane // 16).astype(F32).astype(BF16)
    hi = weight_of.astype(BF16)
    lo = (weight_of - hi.astype(F32)).astype(BF16)
    turned = dot_nt(turn, jnp.concatenate([slot_of, hi, lo], axis=0)).astype(BF16)
    by_col = dot(
        jnp.concatenate([turned[:, n * experts : (n + 1) * experts] for n in range(3)], axis=0),
        spread,
    )
    col = lax.broadcasted_iota(jnp.int32, (ROWS, count), 1)
    token = lax.broadcasted_iota(jnp.int32, (ROWS, count), 0)
    col_slot = col % SLOTS
    held = by_col[:ROWS] == (col_slot + 1).astype(F32)
    is_shared = col_slot == SLOTS - 1
    own_shared = (token == col // 64).astype(F32)
    coef_hi_ref[...] = jnp.where(
        is_shared, own_shared, jnp.where(held, by_col[ROWS : 2 * ROWS], 0.0)
    ).astype(BF16)
    coef_lo_ref[...] = jnp.where(is_shared | ~held, 0.0, by_col[2 * ROWS :]).astype(BF16)


def attention_kernel(
    place_ref,
    bias_hbm,
    lengths_hbm,
    norm_gain_hbm,
    query_gain_hbm,
    key_gain_hbm,
    routes_hbm,
    route_weight_hbm,
    tokens_hbm,
    wq_hbm,
    wk_hbm,
    wv_hbm,
    key_hbm,
    value_hbm,
    wout_hbm,
    out_ref,
    new_keys_hbm,
    new_values_hbm,
    tok_slice_ref,
    pick_ref,
    coef_hi_ref,
    coef_lo_ref,
    bias_buf,
    lengths_buf,
    norm_gain_buf,
    query_gain_buf,
    key_gain_buf,
    routes_buf,
    route_weight_buf,
    tokens_buf,
    wq_buf,
    wk_buf,
    wv_buf,
    key_buf,
    value_buf,
    wout_buf,
    q_buf,
    z_buf,
    w_buf,
    att_buf,
    length_rows,
    new_keys_buf,
    new_values_buf,
    small_sem,
    sem,
    key_sem,
    value_sem,
    out_sem,
):
    a, b = place_ref[0], place_ref[1]
    small = [
        pltpu.make_async_copy(src, dst, small_sem.at[n])
        for n, (src, dst) in enumerate(
            (
                (routes_hbm, routes_buf),
                (route_weight_hbm, route_weight_buf),
                (norm_gain_hbm, norm_gain_buf),
                (query_gain_hbm, query_gain_buf),
                (key_gain_hbm, key_gain_buf),
                (lengths_hbm, lengths_buf),
                (bias_hbm, bias_buf),
            )
        )
    ]
    large = [
        pltpu.make_async_copy(src, dst, sem.at[n])
        for n, (src, dst) in enumerate(
            (
                (tokens_hbm, tokens_buf),
                (wq_hbm, wq_buf),
                (wk_hbm, wk_buf),
                (wv_hbm, wv_buf),
                (wout_hbm, wout_buf),
            )
        )
    ]
    groups = ROWS // GROUP
    key_copies, value_copies = (
        [
            pltpu.make_async_copy(
                src.at[pl.ds(g * GROUP, GROUP)], dst.at[pl.ds(g * GROUP, GROUP)], sems.at[g]
            )
            for g in range(groups)
        ]
        for src, dst, sems in (
            (key_hbm, key_buf, key_sem),
            (value_hbm, value_buf, value_sem),
        )
    )
    for copy in small + large[:2] + key_copies + large[2:4] + value_copies + large[4:]:
        copy.start()

    cache_len = key_buf.shape[1]
    head_size = key_buf.shape[2]
    for copy in small:
        copy.wait()
    route_tables(
        routes_buf[...], route_weight_buf[...], a, pick_ref, coef_hi_ref, coef_lo_ref
    )
    for s in range(ROWS):
        length_rows[s : s + 1, :] = jnp.full((1, LANES), lengths_buf[s], jnp.int32)
    for copy in large[:2]:
        copy.wait()
    normed = rms_rows(tokens_buf[...].astype(F32), norm_gain_buf[...]).astype(BF16)
    q_buf[...] = (
        rms_rows(dot(normed, wq_buf[...]), query_gain_buf[...]).astype(BF16).astype(F32)
    )
    for j in range(TA):
        cols = pl.ds(pl.multiple_of((j * TB + b) * LANES, LANES), LANES)
        tok_slice_ref[j * ROWS : (j + 1) * ROWS, :] = tokens_buf[:, cols].astype(F32)

    for g in range(groups):
        key_copies[g].wait()
        for s in range(g * GROUP, (g + 1) * GROUP):
            z_buf[s : s + 1, :] = dot_nt(q_buf[s : s + 1, :].astype(BF16), key_buf[s])

    for copy in large[2:4]:
        copy.wait()
    new_keys_buf[...] = rms_rows(dot(normed, wk_buf[...]), key_gain_buf[...]).astype(BF16)
    new_values_buf[...] = dot(normed, wv_buf[...]).astype(BF16)
    out_copies = [
        pltpu.make_async_copy(new_keys_buf, new_keys_hbm, out_sem.at[0]),
        pltpu.make_async_copy(new_values_buf, new_values_hbm, out_sem.at[1]),
    ]

    chunks = cache_len // LANES
    after = lax.broadcasted_iota(jnp.int32, (3 * LANES, LANES), 0) % LANES
    upto = lax.broadcasted_iota(jnp.int32, (3 * LANES, LANES), 1)
    later = (after > upto).astype(F32).astype(BF16)
    chunk_lane = lax.broadcasted_iota(jnp.int32, (ROWS, LANES), 1)
    logits = z_buf[...] * head_size ** (-0.5) + bias_buf[0]
    soft = jnp.log1p(jnp.exp(-jnp.abs(logits)))
    log_beta = jnp.minimum(logits, 0.0) - soft
    log_not = jnp.minimum(-logits, 0.0) - soft
    visible = [chunk_lane + c * LANES < length_rows[...] for c in range(chunks)]
    stacked = jnp.concatenate(
        [
            jnp.where(visible[c], log_not[:, c * LANES : (c + 1) * LANES], 0.0)
            for c in range(chunks)
        ],
        axis=0,
    )
    first = stacked.astype(BF16)
    rest = stacked - first.astype(F32)
    second = rest.astype(BF16)
    third = (rest - second.astype(F32)).astype(BF16)
    inner = dot(jnp.concatenate([first, second, third], axis=1), later)
    totals = jnp.sum(stacked, axis=1, keepdims=True)
    carry = jnp.zeros((ROWS, 1), F32)
    for c in reversed(range(chunks)):
        cols = slice(c * LANES, (c + 1) * LANES)
        later_sum = inner[c * ROWS : (c + 1) * ROWS, :] + carry
        w_buf[:, cols] = jnp.where(visible[c], jnp.exp(log_beta[:, cols] + later_sum), 0.0)
        carry = carry + totals[c * ROWS : (c + 1) * ROWS, :]

    for copy in out_copies:
        copy.start()
    for g in range(groups):
        value_copies[g].wait()
        for s in range(g * GROUP, (g + 1) * GROUP):
            att_buf[s : s + 1, :] = dot(w_buf[s : s + 1, :].astype(BF16), value_buf[s])
    large[4].wait()
    attn = dot(att_buf[...].astype(BF16), wout_buf[...]).astype(BF16)
    for t in range(BLOCKS):
        block = attn[:, t * LANES : (t + 1) * LANES]
        j, quarter = t // TB, t % TB
        for n in range(TA):
            start = (n * TB + quarter) * 64 + j * ROWS
            out_ref[start : start + ROWS, :] = block
    for copy in out_copies:
        copy.wait()


def attention(
    place,
    bias,
    lengths,
    norm_gain,
    query_gain,
    key_gain,
    routes,
    route_weight,
    tokens,
    wq,
    wk,
    wv,
    keys,
    values,
    wout,
):
    rows, cache_len, head_size = keys.shape
    width = tokens.shape[1]
    shape = jax.ShapeDtypeStruct
    return pl.pallas_call(
        attention_kernel,
        name="attention",
        out_shape=(
            shape((1024, LANES), BF16),
            shape((rows, head_size), BF16),
            shape((rows, head_size), BF16),
            shape((64, LANES), F32),
            shape((1024, 64), BF16),
            shape((rows, 1024), BF16),
            shape((rows, 1024), BF16),
        ),
        in_specs=[smem()] + [hbm()] * 14,
        out_specs=(vmem(), hbm(), hbm(), vmem(), vmem(), vmem(), vmem()),
        scratch_shapes=[
            pltpu.SMEM(bias.shape, F32),
            pltpu.SMEM(lengths.shape, jnp.int32),
            pltpu.VMEM(norm_gain.shape, F32),
            pltpu.VMEM(query_gain.shape, F32),
            pltpu.VMEM(key_gain.shape, F32),
            pltpu.VMEM(routes.shape, jnp.int32),
            pltpu.VMEM(route_weight.shape, F32),
            pltpu.VMEM((rows, width), BF16),
            pltpu.VMEM((width, head_size), BF16),
            pltpu.VMEM((width, head_size), BF16),
            pltpu.VMEM((width, head_size), BF16),
            pltpu.VMEM((rows, cache_len, head_size), BF16),
            pltpu.VMEM((rows, cache_len, head_size), BF16),
            pltpu.VMEM((head_size, width), BF16),
            pltpu.VMEM((rows, head_size), F32),
            pltpu.VMEM((rows, cache_len), F32),
            pltpu.VMEM((rows, cache_len), F32),
            pltpu.VMEM((rows, head_size), F32),
            pltpu.VMEM((rows, LANES), jnp.int32),
            pltpu.VMEM((rows, head_size), BF16),
            pltpu.VMEM((rows, head_size), BF16),
            pltpu.SemaphoreType.DMA((7,)),
            pltpu.SemaphoreType.DMA((5,)),
            pltpu.SemaphoreType.DMA((rows // GROUP,)),
            pltpu.SemaphoreType.DMA((rows // GROUP,)),
            pltpu.SemaphoreType.DMA((2,)),
        ],
        cost_estimate=pl.CostEstimate(
            flops=2_000_000_000, bytes_accessed=10 * MIB, transcendentals=0
        ),
        compiler_params=pltpu.CompilerParams(vmem_limit_bytes=56 * MIB),
    )(
        place,
        bias,
        lengths,
        norm_gain,
        query_gain,
        key_gain,
        routes,
        route_weight,
        tokens,
        wq,
        wk,
        wv,
        keys,
        values,
        wout,
    )


def dispatch_kernel(place_ref, arrived_ref, tok_slice_ref, pick_ref, out_ref, own_ref, h_buf):
    total = tok_slice_ref[...]
    parts = [arrived_ref[n * 64 : (n + 1) * 64, :].astype(F32) for n in range(TA * TB)]
    while len(parts) > 1:
        parts = [parts[n] + parts[n + 1] for n in range(0, len(parts), 2)]
    h = (total + parts[0]).astype(BF16)
    h_buf[...] = h.astype(F32)
    out_ref[...] = dot(pick_ref[...], h).astype(BF16)
    own_ref[...] = h_buf[pl.ds(pl.multiple_of(place_ref[0] * ROWS, ROWS), ROWS), :]


def dispatch(place, arrived, tok_slice, pick):
    shape = jax.ShapeDtypeStruct
    return pl.pallas_call(
        dispatch_kernel,
        name="dispatch",
        out_shape=(shape((1024, LANES), BF16), shape((ROWS, LANES), F32)),
        in_specs=[smem()] + [vmem()] * 3,
        out_specs=(vmem(),) * 2,
        scratch_shapes=[pltpu.VMEM((64, LANES), F32)],
        cost_estimate=pl.CostEstimate(
            flops=500_000_000, bytes_accessed=MIB, transcendentals=0
        ),
        compiler_params=pltpu.CompilerParams(vmem_limit_bytes=4 * MIB),
    )(place, arrived, tok_slice, pick)


def expert_kernel(
    arrived_ref,
    post_gain_ref,
    gate_ref,
    up_ref,
    down_ref,
    shared_gate_ref,
    shared_up_ref,
    shared_down_ref,
    out_ref,
    rows_buf,
    x_buf,
    send_buf,
):
    rows_buf[...] = arrived_ref[...].astype(F32)
    for t in range(BLOCKS):
        j, b = t // TB, t % TB
        for s in range(SLOTS):
            x_buf[s * ROWS : (s + 1) * ROWS, t * LANES : (t + 1) * LANES] = rows_buf[
                pl.ds(b * 16 + j * SLOTS + s, EP, stride=64), :
            ]
    h_normed = rms_rows(x_buf[...], post_gain_ref[...]).astype(BF16)
    routed_rows, shared_rows = h_normed[:48], h_normed[48:]
    gate = dot(routed_rows, gate_ref[...])
    up = dot(routed_rows, up_ref[...])
    hidden = (gate * jax.nn.sigmoid(gate) * up).astype(BF16)
    s_gate = dot_nt(shared_rows, shared_gate_ref[...])
    s_up = dot_nt(shared_rows, shared_up_ref[...])
    s_hidden = (s_gate * jax.nn.sigmoid(s_gate) * s_up).astype(BF16)
    routed = dot(hidden, down_ref[...])
    shared = dot(s_hidden, shared_down_ref[...])
    for t in range(BLOCKS):
        cols = slice(t * LANES, (t + 1) * LANES)
        for s in range(SLOTS):
            part = routed[s * ROWS : (s + 1) * ROWS, cols] if s < SLOTS - 1 else shared[:, cols]
            send_buf[pl.ds(t * SLOTS + s, EP, stride=64), :] = part
    out_ref[...] = send_buf[...].astype(BF16)


def run_experts(arrived, post_gain, gate, up, down, s_gate, s_up, s_down):
    return pl.pallas_call(
        expert_kernel,
        name="experts",
        out_shape=jax.ShapeDtypeStruct((1024, LANES), BF16),
        in_specs=[vmem()] * 8,
        out_specs=vmem(),
        scratch_shapes=[
            pltpu.VMEM((1024, LANES), F32),
            pltpu.VMEM((64, BLOCKS * LANES), F32),
            pltpu.VMEM((1024, LANES), F32),
        ],
        cost_estimate=pl.CostEstimate(
            flops=1_000_000_000, bytes_accessed=3 * MIB, transcendentals=0
        ),
        compiler_params=pltpu.CompilerParams(vmem_limit_bytes=12 * MIB),
    )(arrived, post_gain, gate, up, down, s_gate, s_up, s_down)


def combine_kernel(arrived_ref, coef_hi_ref, coef_lo_ref, own_ref, out_ref):
    arrived = arrived_ref[...]
    both = dot(jnp.concatenate([coef_hi_ref[...], coef_lo_ref[...]], axis=0), arrived)
    out_ref[...] = (own_ref[...] + (both[:ROWS] + both[ROWS:])).astype(BF16)


def combine(arrived, coef_hi, coef_lo, own):
    return pl.pallas_call(
        combine_kernel,
        name="combine",
        out_shape=jax.ShapeDtypeStruct((ROWS, LANES), BF16),
        in_specs=[vmem()] * 4,
        out_specs=vmem(),
        cost_estimate=pl.CostEstimate(
            flops=100_000_000, bytes_accessed=MIB, transcendentals=0
        ),
        compiler_params=pltpu.CompilerParams(vmem_limit_bytes=4 * MIB),
    )(arrived, coef_hi, coef_lo, own)


def exchange(x, axes, parts):
    pieces = x.reshape(parts, -1, LANES)
    arrived = lax.all_to_all(pieces, axes, split_axis=0, concat_axis=0, tiled=True)
    return arrived.reshape(x.shape)


def local(
    tokens,
    norm_gain,
    w_query,
    w_key,
    w_value,
    query_gain,
    key_gain,
    score_bias,
    key_cache,
    value_cache,
    lengths,
    w_out,
    post_gain,
    routes,
    route_weight,
    expert_gate,
    expert_up,
    expert_down,
    shared_gate,
    shared_up,
    shared_down,
):
    place = jnp.stack([lax.axis_index("ta"), lax.axis_index("tb")]).astype(jnp.int32)
    partial_rows, new_keys, new_values, tok_slice, pick, coef_hi, coef_lo = attention(
        place,
        score_bias,
        lengths,
        norm_gain[None, :],
        query_gain[None, :],
        key_gain[None, :],
        routes.T,
        route_weight.T,
        tokens,
        w_query,
        w_key,
        w_value,
        key_cache,
        value_cache,
        w_out,
    )
    arrived = exchange(partial_rows, ("ta", "tb"), TA * TB)
    outgoing, own = dispatch(place, arrived, tok_slice, pick)
    received = exchange(outgoing, ("ep", "tb"), EP * TB)
    parts = run_experts(
        received,
        post_gain[None, :],
        expert_gate[0],
        expert_up[0],
        expert_down[0],
        shared_gate.T,
        shared_up.T,
        shared_down,
    )
    returned = exchange(parts, ("ep", "ta", "tb"), EP * TA * TB)
    mixed = combine(returned, coef_hi, coef_lo, own)
    return (mixed, new_keys, new_values)


def solution(mesh):
    cut = Mesh(mesh.devices.reshape(EP, TA, TB), ("ep", "ta", "tb"))
    tp = ("ta", "tb")
    placed = (
        P("ep", None),
        P(),
        P(None, tp),
        P(None, tp),
        P(None, tp),
        P(),
        P(),
        P(tp),
        P("ep", None, tp),
        P("ep", None, tp),
        P("ep"),
        P(tp, None),
        P(),
        P("ep", None),
        P("ep", None),
        P(("ep", "ta", "tb"), None, None),
        P(("ep", "ta", "tb"), None, None),
        P(("ep", "ta", "tb"), None, None),
        P(None, tp),
        P(None, tp),
        P(tp, None),
    )
    return jax.shard_map(
        local,
        mesh=cut,
        in_specs=placed,
        out_specs=(P("ep", tp),) * 3,
        check_vma=False,
    )
```

time: 114 us -> 75.5 us (0.66)
  blocking collectives: 0 us -> 60.7 us
  waiting for transfers between devices: 42.4 us -> 0 us
  starting transfers between devices: 28.9 us -> 0 us
  other arithmetic: 24 us -> 0.61 us
  matrix products: 11.6 us -> 0 us
  Pallas kernels: 0 us -> 10.7 us
  local copies, waits for them, and re-layouts: 5 us -> 1.76 us
    all_to_all x0 -> x3, blocking collectives: none -> 60.7 us  [exchange(): lax.all_to_all(pieces, axes, split_axis=0, concat_axis=0, tiled=True)]
    all_to_all x5 -> x0, waiting for transfers between devices: 42.4 us -> none  [the longest x2 15.7 us: sent_and_summed(): lax.all_to_all(pieces, axis, split_axis=0, concat_axis=0, tiled=True)]
    all_to_all x5 -> x0, starting transfers between devices: 28.9 us -> none  [the longest x2 15.2 us: sent_and_summed(): lax.all_to_all(pieces, axis, split_axis=0, concat_axis=0, tiled=True)]
    another operation x3 -> x1, other arithmetic: 20 us -> 0.61 us  [local(): jnp.stack([lax.axis_index('ta'), lax.axis_index('tb')]).astype(jnp.int32)]
    dot_general x14 -> x0, matrix products: 11.6 us -> none  [the longest x1 3.42 us: local(): jnp.einsum('shd,slhd->shl', queries, key_blocks, preferred_element_type=j...]
    pallas_call x0 -> x4, Pallas kernels: none -> 10.7 us  [the longest x1 8.05 us: attention(): pl.pallas_call(attention_kernel, name='attention', out_shape=(shape((1024...]
    reshape x7 -> x0, local copies, waits for them, and re-layouts: 2.58 us -> none  [the longest x2 1.43 us: cut_along(): return jnp.moveaxis(x.reshape(*before, devices, -1, *after), dim, 0)]
    convert_element_type x6 -> x0, other arithmetic: 2.24 us -> none  [the longest x1 0.73 us: local(): queries = rms_scale(queries, query_gain).astype(jnp.bfloat16)]
  transfers between devices with their start and end apart: 5 -> 0, of which waited for: 5 -> 0; matrix products, arithmetic and copies ran while one was open for 3% -> 0% of each run, Pallas kernels for 0% -> 0%
where the time goes in v1:
time: 75.5 us; the launch traced here: 75.1 us
  blocking collectives  60.7 us (80%)
  Pallas kernels  10.7 us (14%)
  local copies, waits for them, and re-layouts  1.76 us (2%)
  between operations  1.4 us (2%)
    all_to_all x3, blocking collectives, exchange(): lax.all_to_all(pieces, axes, split_axis=0, concat_axis=0, tiled=True)  60.7 us
    pallas_call x1, Pallas kernels, attention(): pl.pallas_call(attention_kernel, name='attention', out_shape=(shape((1024...  8.05 us
    unnamed x24, local copies, waits for them, and re-layouts  1.76 us

profile of v1, /device:TPU:1, one launch (start us, length us, event | category | flops | bytes accessed | tf_op | source)
XLA Modules:
  0.0 75.1 jit_solution(6832528784102555695)
XLA Ops:
  1.3 0.6 pad_add_fusion.place_ref
  1.9 0.0 copy-start.5
  1.9 0.0 copy-start.6
  1.9 0.0 copy-start.7
  1.9 0.0 copy-start.11
  1.9 8.1 %attention.1 = (bf16[1024,128]{1,0:T(8,128)(2,1)}, bf16[16,128]{1,0:T(8,128)(2,1)}, bf16[16,128]{1,0:T(8,128)(2,1)}, f32[64,128]{1,0:T(8,128)}, bf16[1024,64]{1,...) custom-call(s32[2]{0:T(128)} %pad_add_fusion.place_ref, f32[1]{0:T(128)S(6)} %copy.24.bias_hbm, ...), custom_call_target="tpu_custom_call" | custom-call | flops 2000000000 | bytes 10485760 | tf_op jit(solution)/shard_map/attention/pallas_call | solution.py:291
  10.0 0.0 copy-start.8
  10.0 0.0 copy-start.9
  10.0 21.6 %all_to_all.15 = bf16[16,64,128]{2,1,0:T(8,128)(2,1)S(1)} all-to-all(bf16[16,64,128]{2,1,0:T(8,128)(2,1)} %bitcast.30), channel_id=1, replica_groups=mesh['ep'=16,'ta'=4,'tb'=4] {'ta','tb'}, dimensions={0} | all-to-all | bytes 524288 | tf_op jit(solution)/shard_map/all_to_all | solution.py:463
  31.6 0.0 copy-done
  31.6 0.9 %copy-done.4 = bf16[1024,64]{1,0:T(8,128)(2,1)S(1)} copy-done((bf16[1024,64]{1,0:T(8,128)(2,1)S(1)}, bf16[1024,64]{1,0:T(8,128)(2,1)}, u32[]{:S(2)}) %copy-start.4) | copy-done | bytes 131096
  32.5 0.8 %copy-done.10 = f32[64,128]{1,0:T(8,128)S(1)} copy-done((f32[64,128]{1,0:T(8,128)S(1)}, f32[64,128]{1,0:T(8,128)}, u32[]{:S(2)}) %copy-start.10) | copy-done | bytes 32792
  33.3 0.8 %dispatch.1 = (bf16[1024,128]{1,0:T(8,128)(2,1)S(1)}, f32[16,128]{1,0:T(8,128)S(1)}) custom-call(s32[2]{0:T(128)S(1)} %copy-done, bf16[1024,128]{1,0:T(8,128)(2,1)S(1)} %bitcast.19, f32[64,128]{1,0:T(8,128)S(1)} %copy-done.10, bf16[1024,64]{1,0:T(8,128)(2,1)S(1)} %copy-done.4), custom_call_target="tpu_custom_call" | custom-call | flops 500000000 | bytes 1048576 | tf_op jit(solution)/shard_map/dispatch/pallas_call | solution.py:369
  34.1 17.4 %all_to_all.16 = bf16[64,16,128]{2,1,0:T(8,128)(2,1)S(1)} all-to-all(bf16[64,16,128]{2,1,0:T(8,128)(2,1)S(1)} %bitcast.20), channel_id=1, replica_groups=mesh['ep'=16,'ta'=4,'tb'=4] {'ep','tb'}, dimensions={0} | all-to-all | bytes 524288 | tf_op jit(solution)/shard_map/all_to_all | solution.py:463
  51.4 0.0 copy-done.1
  51.4 0.0 copy-done.2
  51.5 0.0 copy-done.5
  51.5 0.0 copy-done.6
  51.5 0.0 copy-done.7
  51.5 0.0 copy-done.11
  51.5 1.1 %experts.1 = bf16[1024,128]{1,0:T(8,128)(2,1)S(1)} custom-call(bf16[1024,128]{1,0:T(8,128)(2,1)S(1)} %bitcast.22, f32[1,2048]{1,0:T(1,128)S(1)} %bitcast.29, bf16[2048,128]{1,0:T(8,128)(2,1)S(1)} %bitcast.24, bf16[2048,128]{1,0:T(8,128)(2,1)S(1)} %bitcast.25, bf16[128,2048]{1,0:T(8,128)(2,1)S(1)} %bitcast.26, bf16[32,2048]{1,0:T(8,128)(2,1)S(1)} %bitcast.27, ...), custom_call_target="tpu_custom_call" | custom-call | flops 1000000000 | bytes 3145728 | tf_op jit(solution)/shard_map/experts/pallas_call | solution.py:423
  52.6 21.8 %all_to_all.17 = bf16[256,4,128]{2,1,0:T(4,128)(2,1)S(1)} all-to-all(bf16[256,4,128]{2,1,0:T(4,128)(2,1)S(1)} %bitcast.23), channel_id=1, replica_groups=mesh['ep'=16,'ta'=4,'tb'=4] {'ep','ta','tb'}, dimensions={0} | all-to-all | bytes 524288 | tf_op jit(solution)/shard_map/all_to_all | solution.py:463
  74.4 0.0 copy-done.8
  74.4 0.8 %combine.1 = bf16[16,128]{1,0:T(8,128)(2,1)} custom-call(bf16[1024,128]{1,0:T(8,128)(2,1)S(1)} %bitcast.21, bf16[16,1024]{1,0:T(8,128)(2,1)S(1)} %copy-done.8, bf16[16,1024]{1,0:T(8,128)(2,1)S(1)} %copy-done.9, f32[16,128]{1,0:T(8,128)S(1)} %get-tuple-element.18.own_ref), custom_call_target="tpu_custom_call" | custom-call | flops 100000000 | bytes 1048576 | tf_op jit(solution)/shard_map/combine/pallas_call | solution.py:448
  (8 shorter events, 0.0 us)
Async XLA Ops:
  1.9 29.7 %copy-start = (s32[2]{0:T(128)S(1)}, s32[2]{0:T(128)}, u32[]{:S(2)}) copy-start(s32[2]{0:T(128)} %pad_add_fusion.place_ref) | copy-start | bytes 28
  1.9 49.6 %copy-start.1 = (bf16[1,2048,128]{2,1,0:T(8,128)(2,1)S(1)}, bf16[1,2048,128]{2,1,0:T(8,128)(2,1)}, u32[]{:S(2)}) copy-start(bf16[1,2048,128]{2,1,0:T(8,128)(2,1)} %param.36) | copy-start | bytes 1572868
  1.9 49.6 %copy-start.2 = (bf16[1,2048,128]{2,1,0:T(8,128)(2,1)S(1)}, bf16[1,2048,128]{2,1,0:T(8,128)(2,1)}, u32[]{:S(2)}) copy-start(bf16[1,2048,128]{2,1,0:T(8,128)(2,1)} %param.37) | copy-start | bytes 1572868
  1.9 49.6 %copy-start.3 = (bf16[1,128,2048]{2,1,0:T(8,128)(2,1)S(1)}, bf16[1,128,2048]{2,1,0:T(8,128)(2,1)}, u32[]{:S(2)}) copy-start(bf16[1,128,2048]{2,1,0:T(8,128)(2,1)} %param.38) | copy-start | bytes 1572868
  1.9 49.6 %copy-start.5 = (bf16[2048,32]{0,1:T(8,128)(2,1)S(1)}, bf16[2048,32]{0,1:T(8,128)(2,1)}, u32[]{:S(2)}) copy-start(bf16[2048,32]{0,1:T(8,128)(2,1)} %param.39) | copy-start | bytes 393220
  1.9 49.6 %copy-start.6 = (bf16[2048,32]{0,1:T(8,128)(2,1)S(1)}, bf16[2048,32]{0,1:T(8,128)(2,1)}, u32[]{:S(2)}) copy-start(bf16[2048,32]{0,1:T(8,128)(2,1)} %param.40) | copy-start | bytes 393220
  1.9 49.6 %copy-start.7 = (bf16[32,2048]{1,0:T(8,128)(2,1)S(1)}, bf16[32,2048]{1,0:T(8,128)(2,1)}, u32[]{:S(2)}) copy-start(bf16[32,2048]{1,0:T(8,128)(2,1)} %shared_down_ref.1) | copy-start | bytes 393220
  1.9 49.5 %copy-start.11 = (f32[2048]{0:T(1024)S(1)}, f32[2048]{0:T(1024)}, u32[]{:S(2)}) copy-start(f32[2048]{0:T(1024)} %param.33) | copy-start | bytes 24580
  10.0 64.3 %copy-start.8 = (bf16[16,1024]{1,0:T(8,128)(2,1)S(1)}, bf16[16,1024]{1,0:T(8,128)(2,1)}, u32[]{:S(2)}) copy-start(bf16[16,1024]{1,0:T(8,128)(2,1)} %get-tuple-element.16.coef_hi_ref) | copy-start | bytes 98308
  10.0 64.3 %copy-start.9 = (bf16[16,1024]{1,0:T(8,128)(2,1)S(1)}, bf16[16,1024]{1,0:T(8,128)(2,1)}, u32[]{:S(2)}) copy-start(bf16[16,1024]{1,0:T(8,128)(2,1)} %get-tuple-element.17.coef_lo_ref) | copy-start | bytes 98308
  31.6 1.0 %copy-start.4 = (bf16[1024,64]{1,0:T(8,128)(2,1)S(1)}, bf16[1024,64]{1,0:T(8,128)(2,1)}, u32[]{:S(2)}) copy-start(bf16[1024,64]{1,0:T(8,128)(2,1)} %get-tuple-element.14.pick_ref) | copy-start | bytes 393220
  32.5 0.8 %copy-start.10 = (f32[64,128]{1,0:T(8,128)S(1)}, f32[64,128]{1,0:T(8,128)}, u32[]{:S(2)}) copy-start(f32[64,128]{1,0:T(8,128)} %get-tuple-element.13.tok_slice_ref) | copy-start | bytes 98308

commit v2 on v1

--- a/solution.py
+++ b/solution.py
@@ -13,6 +13,8 @@
 ROWS = 16
 SLOTS = 4
 GROUP = 4
+HEAD_ROWS = 256
+TILE = 16
 BLOCKS = 16
 MIB = 1024 * 1024
 
@@ -32,10 +34,6 @@
 
 def vmem():
     return pl.BlockSpec(memory_space=pltpu.VMEM)
-
-
-def smem():
-    return pl.BlockSpec(memory_space=pltpu.SMEM)
 
 
 def hbm():
@@ -95,7 +93,6 @@
 
 
 def attention_kernel(
-    place_ref,
     bias_hbm,
     lengths_hbm,
     norm_gain_hbm,
@@ -144,18 +141,18 @@
     value_sem,
     out_sem,
 ):
-    a, b = place_ref[0], place_ref[1]
+    a, b = lax.axis_index("ta"), lax.axis_index("tb")
     small = [
         pltpu.make_async_copy(src, dst, small_sem.at[n])
         for n, (src, dst) in enumerate(
             (
+                (lengths_hbm, lengths_buf),
+                (bias_hbm, bias_buf),
                 (routes_hbm, routes_buf),
                 (route_weight_hbm, route_weight_buf),
                 (norm_gain_hbm, norm_gain_buf),
                 (query_gain_hbm, query_gain_buf),
                 (key_gain_hbm, key_gain_buf),
-                (lengths_hbm, lengths_buf),
-                (bias_hbm, bias_buf),
             )
         )
     ]
@@ -171,25 +168,35 @@
             )
         )
     ]
-    groups = ROWS // GROUP
-    key_copies, value_copies = (
-        [
-            pltpu.make_async_copy(
-                src.at[pl.ds(g * GROUP, GROUP)], dst.at[pl.ds(g * GROUP, GROUP)], sems.at[g]
-            )
-            for g in range(groups)
-        ]
-        for src, dst, sems in (
-            (key_hbm, key_buf, key_sem),
-            (value_hbm, value_buf, value_sem),
-        )
-    )
-    for copy in small + large[:2] + key_copies + large[2:4] + value_copies + large[4:]:
-        copy.start()
-
     cache_len = key_buf.shape[1]
     head_size = key_buf.shape[2]
-    for copy in small:
+    caches = ((key_hbm, key_buf, key_sem), (value_hbm, value_buf, value_sem))
+    head_copies = [
+        pltpu.make_async_copy(
+            src.at[:, pl.ds(0, HEAD_ROWS)], dst.at[:, pl.ds(0, HEAD_ROWS)], sems.at[ROWS]
+        )
+        for src, dst, sems in caches
+    ]
+    for copy in small + large[:2] + head_copies[:1]:
+        copy.start()
+    value_buf[:, HEAD_ROWS:, :] = jnp.zeros(
+        (ROWS, cache_len - HEAD_ROWS, head_size), value_buf.dtype
+    )
+    small[0].wait()
+    small[1].wait()
+
+    def tail_copy(cache, s):
+        src, dst, sems = cache
+        tiles = jnp.maximum((lengths_buf[s] + TILE - 1) // TILE, HEAD_ROWS // TILE + 1)
+        size = pl.multiple_of((tiles - HEAD_ROWS // TILE) * TILE, TILE)
+        part = pl.ds(HEAD_ROWS, size)
+        return pltpu.make_async_copy(src.at[s, part], dst.at[s, part], sems.at[s])
+
+    key_copies, value_copies = ([tail_copy(cache, s) for s in range(ROWS)] for cache in caches)
+    for copy in key_copies + head_copies[1:]:
+        copy.start()
+
+    for copy in small[2:]:
         copy.wait()
     route_tables(
         routes_buf[...], route_weight_buf[...], a, pick_ref, coef_hi_ref, coef_lo_ref
@@ -206,11 +213,18 @@
         cols = pl.ds(pl.multiple_of((j * TB + b) * LANES, LANES), LANES)
         tok_slice_ref[j * ROWS : (j + 1) * ROWS, :] = tokens_buf[:, cols].astype(F32)
 
-    for g in range(groups):
-        key_copies[g].wait()
-        for s in range(g * GROUP, (g + 1) * GROUP):
+    head_copies[0].wait()
+    for g in range(ROWS // GROUP):
+        members = range(g * GROUP, (g + 1) * GROUP)
+        for s in members:
+            key_copies[s].wait()
+        for s in members:
+            value_copies[s].start()
+        for s in members:
             z_buf[s : s + 1, :] = dot_nt(q_buf[s : s + 1, :].astype(BF16), key_buf[s])
 
+    for copy in large[2:]:
+        copy.start()
     for copy in large[2:4]:
         copy.wait()
     new_keys_buf[...] = rms_rows(dot(normed, wk_buf[...]), key_gain_buf[...]).astype(BF16)
@@ -225,7 +239,7 @@
     upto = lax.broadcasted_iota(jnp.int32, (3 * LANES, LANES), 1)
     later = (after > upto).astype(F32).astype(BF16)
     chunk_lane = lax.broadcasted_iota(jnp.int32, (ROWS, LANES), 1)
-    logits = z_buf[...] * head_size ** (-0.5) + bias_buf[0]
+    logits = z_buf[...] * head_size ** (-0.5) + bias_buf[0, 0]
     soft = jnp.log1p(jnp.exp(-jnp.abs(logits)))
     log_beta = jnp.minimum(logits, 0.0) - soft
     log_not = jnp.minimum(-logits, 0.0) - soft
@@ -252,9 +266,12 @@
 
     for copy in out_copies:
         copy.start()
-    for g in range(groups):
-        value_copies[g].wait()
-        for s in range(g * GROUP, (g + 1) * GROUP):
+    head_copies[1].wait()
+    for g in range(ROWS // GROUP):
+        members = range(g * GROUP, (g + 1) * GROUP)
+        for s in members:
+            value_copies[s].wait()
+        for s in members:
             att_buf[s : s + 1, :] = dot(w_buf[s : s + 1, :].astype(BF16), value_buf[s])
     large[4].wait()
     attn = dot(att_buf[...].astype(BF16), wout_buf[...]).astype(BF16)
@@ -269,7 +286,6 @@
 
 
 def attention(
-    place,
     bias,
     lengths,
     norm_gain,
@@ -300,7 +316,7 @@
             shape((rows, 1024), BF16),
             shape((rows, 1024), BF16),
         ),
-        in_specs=[smem()] + [hbm()] * 14,
+        in_specs=[hbm()] * 14,
         out_specs=(vmem(), hbm(), hbm(), vmem(), vmem(), vmem(), vmem()),
         scratch_shapes=[
             pltpu.SMEM(bias.shape, F32),
@@ -326,17 +342,17 @@
             pltpu.VMEM((rows, head_size), BF16),
             pltpu.SemaphoreType.DMA((7,)),
             pltpu.SemaphoreType.DMA((5,)),
-            pltpu.SemaphoreType.DMA((rows // GROUP,)),
-            pltpu.SemaphoreType.DMA((rows // GROUP,)),
+            pltpu.SemaphoreType.DMA((rows + 1,)),
+            pltpu.SemaphoreType.DMA((rows + 1,)),
             pltpu.SemaphoreType.DMA((2,)),
         ],
         cost_estimate=pl.CostEstimate(
             flops=2_000_000_000, bytes_accessed=10 * MIB, transcendentals=0
         ),
-        compiler_params=pltpu.CompilerParams(vmem_limit_bytes=56 * MIB),
+        compiler_params=pltpu.CompilerParams(vmem_limit_bytes=16 * MIB),
     )(
-        place,
         bias,
+        *(pltpu.with_memory_space_constraint(x, pltpu.HBM) for x in (
         lengths,
         norm_gain,
         query_gain,
@@ -350,10 +366,11 @@
         keys,
         values,
         wout,
-    )
-
-
-def dispatch_kernel(place_ref, arrived_ref, tok_slice_ref, pick_ref, out_ref, own_ref, h_buf):
+        ))
+    )
+
+
+def dispatch_kernel(arrived_ref, tok_slice_ref, pick_ref, out_ref, own_ref, h_buf):
     total = tok_slice_ref[...]
     parts = [arrived_ref[n * 64 : (n + 1) * 64, :].astype(F32) for n in range(TA * TB)]
     while len(parts) > 1:
@@ -361,23 +378,23 @@
     h = (total + parts[0]).astype(BF16)
     h_buf[...] = h.astype(F32)
     out_ref[...] = dot(pick_ref[...], h).astype(BF16)
-    own_ref[...] = h_buf[pl.ds(pl.multiple_of(place_ref[0] * ROWS, ROWS), ROWS), :]
-
-
-def dispatch(place, arrived, tok_slice, pick):
+    own_ref[...] = h_buf[pl.ds(pl.multiple_of(lax.axis_index("ta") * ROWS, ROWS), ROWS), :]
+
+
+def dispatch(arrived, tok_slice, pick):
     shape = jax.ShapeDtypeStruct
     return pl.pallas_call(
         dispatch_kernel,
         name="dispatch",
         out_shape=(shape((1024, LANES), BF16), shape((ROWS, LANES), F32)),
-        in_specs=[smem()] + [vmem()] * 3,
+        in_specs=[vmem()] * 3,
         out_specs=(vmem(),) * 2,
         scratch_shapes=[pltpu.VMEM((64, LANES), F32)],
         cost_estimate=pl.CostEstimate(
             flops=500_000_000, bytes_accessed=MIB, transcendentals=0
         ),
         compiler_params=pltpu.CompilerParams(vmem_limit_bytes=4 * MIB),
-    )(place, arrived, tok_slice, pick)
+    )(arrived, tok_slice, pick)
 
 
 def expert_kernel(
@@ -487,10 +504,8 @@
     shared_up,
     shared_down,
 ):
-    place = jnp.stack([lax.axis_index("ta"), lax.axis_index("tb")]).astype(jnp.int32)
     partial_rows, new_keys, new_values, tok_slice, pick, coef_hi, coef_lo = attention(
-        place,
-        score_bias,
+        score_bias[None, :],
         lengths,
         norm_gain[None, :],
         query_gain[None, :],
@@ -505,8 +520,11 @@
         value_cache,
         w_out,
     )
+    later = (post_gain, expert_gate, expert_up, expert_down, shared_gate, shared_up, shared_down)
+    partial_rows, *later = lax.optimization_barrier((partial_rows, *later))
+    post_gain, expert_gate, expert_up, expert_down, shared_gate, shared_up, shared_down = later
     arrived = exchange(partial_rows, ("ta", "tb"), TA * TB)
-    outgoing, own = dispatch(place, arrived, tok_slice, pick)
+    outgoing, own = dispatch(arrived, tok_slice, pick)
     received = exchange(outgoing, ("ep", "tb"), EP * TB)
     parts = run_experts(
         received,

time: 75.5 us -> 71.1 us (0.942)
  local copies, waits for them, and re-layouts: 1.76 us -> 0.03 us
  Pallas kernels: 10.7 us -> 9.04 us
    unnamed x24 -> x14, local copies, waits for them, and re-layouts: 1.76 us -> 0.03 us
    pallas_call x1, Pallas kernels: 8.05 us -> 6.97 us  [attention(): pl.pallas_call(attention_kernel, name='attention', out_shape=(shape((1024...]
where the time goes in v2:
time: 71.1 us; the launch traced here: 71 us
  blocking collectives  60.5 us (85%)
  Pallas kernels  9.04 us (13%)
  between operations  1.4 us (2%)
    all_to_all x3, blocking collectives, exchange(): lax.all_to_all(pieces, axes, split_axis=0, concat_axis=0, tiled=True)  60.5 us
    pallas_call x1, Pallas kernels, attention(): pl.pallas_call(attention_kernel, name='attention', out_shape=(shape((1024...  6.97 us

profile of v2, /device:TPU:1, one launch (start us, length us, event | category | flops | bytes accessed | tf_op | source)
XLA Modules:
  0.0 71.0 jit_solution(7831537804928045920)
XLA Ops:
  1.3 0.0 copy-start
  1.3 0.0 copy-start.1
  1.3 0.0 copy-start.2
  1.3 0.0 copy-start.3
  1.3 0.0 copy-start.4
  1.3 0.0 copy-start.5
  1.3 0.0 copy-start.6
  1.4 7.0 %attention.1 = (bf16[1024,128]{1,0:T(8,128)(2,1)S(1)}, bf16[16,128]{1,0:T(8,128)(2,1)}, bf16[16,128]{1,0:T(8,128)(2,1)}, f32[64,128]{1,0:T(8,128)S(1)}, bf16[102...) custom-call(f32[1,1]{1,0:T(1,128)} %bitcast.18.bias_hbm, s32[16]{0:T(128)} %lengths_hbm.1, ...), custom_call_target="tpu_custom_call" | custom-call | flops 2000000000 | bytes 10485760 | tf_op jit(solution)/shard_map/attention/pallas_call | solution.py:307
  8.3 21.4 %all_to_all.15 = bf16[16,64,128]{2,1,0:T(8,128)(2,1)S(1)} all-to-all(bf16[16,64,128]{2,1,0:T(8,128)(2,1)S(1)} %bitcast.19), channel_id=1, replica_groups=mesh['ep'=16,'ta'=4,'tb'=4] {'ta','tb'}, dimensions={0} | all-to-all | bytes 524288 | tf_op jit(solution)/shard_map/all_to_all | solution.py:480
  29.7 0.2 dispatch.1
  29.9 17.4 %all_to_all.16 = bf16[64,16,128]{2,1,0:T(8,128)(2,1)S(1)} all-to-all(bf16[64,16,128]{2,1,0:T(8,128)(2,1)S(1)} %bitcast.21), channel_id=1, replica_groups=mesh['ep'=16,'ta'=4,'tb'=4] {'ep','tb'}, dimensions={0} | all-to-all | bytes 524288 | tf_op jit(solution)/shard_map/all_to_all | solution.py:480
  47.3 0.0 copy-done
  47.3 0.0 copy-done.1
  47.3 0.0 copy-done.2
  47.3 0.0 copy-done.3
  47.3 0.0 copy-done.4
  47.3 0.0 copy-done.5
  47.3 0.0 copy-done.6
  47.3 1.1 %experts.1 = bf16[1024,128]{1,0:T(8,128)(2,1)S(1)} custom-call(bf16[1024,128]{1,0:T(8,128)(2,1)S(1)} %bitcast.23, f32[1,2048]{1,0:T(1,128)S(1)} %bitcast.30, bf16[2048,128]{1,0:T(8,128)(2,1)S(1)} %bitcast.25, bf16[2048,128]{1,0:T(8,128)(2,1)S(1)} %bitcast.26, bf16[128,2048]{1,0:T(8,128)(2,1)S(1)} %bitcast.27, bf16[32,2048]{1,0:T(8,128)(2,1)S(1)} %bitcast.28, ...), custom_call_target="tpu_custom_call" | custom-call | flops 1000000000 | bytes 3145728 | tf_op jit(solution)/shard_map/experts/pallas_call | solution.py:440
  48.4 21.8 %all_to_all.17 = bf16[256,4,128]{2,1,0:T(4,128)(2,1)S(1)} all-to-all(bf16[256,4,128]{2,1,0:T(4,128)(2,1)S(1)} %bitcast.24), channel_id=1, replica_groups=mesh['ep'=16,'ta'=4,'tb'=4] {'ep','ta','tb'}, dimensions={0} | all-to-all | bytes 524288 | tf_op jit(solution)/shard_map/all_to_all | solution.py:480
  70.2 0.8 %combine.1 = bf16[16,128]{1,0:T(8,128)(2,1)} custom-call(bf16[1024,128]{1,0:T(8,128)(2,1)S(1)} %bitcast.22, bf16[16,1024]{1,0:T(8,128)(2,1)S(1)} %get-tuple-element.32.coef_hi_ref, bf16[16,1024]{1,0:T(8,128)(2,1)S(1)} %get-tuple-element.33.coef_lo_ref, f32[16,128]{1,0:T(8,128)S(1)} %get-tuple-element.34.own_ref), custom_call_target="tpu_custom_call" | custom-call | flops 100000000 | bytes 1048576 | tf_op jit(solution)/shard_map/combine/pallas_call | solution.py:465
Async XLA Ops:
  1.3 46.0 %copy-start = (bf16[1,2048,128]{2,1,0:T(8,128)(2,1)S(1)}, bf16[1,2048,128]{2,1,0:T(8,128)(2,1)}, u32[]{:S(2)}) copy-start(bf16[1,2048,128]{2,1,0:T(8,128)(2,1)} %param.36) | copy-start | bytes 1572868
  1.3 46.0 %copy-start.1 = (bf16[1,2048,128]{2,1,0:T(8,128)(2,1)S(1)}, bf16[1,2048,128]{2,1,0:T(8,128)(2,1)}, u32[]{:S(2)}) copy-start(bf16[1,2048,128]{2,1,0:T(8,128)(2,1)} %param.37) | copy-start | bytes 1572868
  1.3 46.0 %copy-start.2 = (bf16[1,128,2048]{2,1,0:T(8,128)(2,1)S(1)}, bf16[1,128,2048]{2,1,0:T(8,128)(2,1)}, u32[]{:S(2)}) copy-start(bf16[1,128,2048]{2,1,0:T(8,128)(2,1)} %param.38) | copy-start | bytes 1572868
  1.3 46.0 %copy-start.3 = (bf16[2048,32]{0,1:T(8,128)(2,1)S(1)}, bf16[2048,32]{0,1:T(8,128)(2,1)}, u32[]{:S(2)}) copy-start(bf16[2048,32]{0,1:T(8,128)(2,1)} %param.39) | copy-start | bytes 393220
  1.3 46.0 %copy-start.4 = (bf16[2048,32]{0,1:T(8,128)(2,1)S(1)}, bf16[2048,32]{0,1:T(8,128)(2,1)}, u32[]{:S(2)}) copy-start(bf16[2048,32]{0,1:T(8,128)(2,1)} %param.40) | copy-start | bytes 393220
  1.3 46.0 %copy-start.5 = (bf16[32,2048]{1,0:T(8,128)(2,1)S(1)}, bf16[32,2048]{1,0:T(8,128)(2,1)}, u32[]{:S(2)}) copy-start(bf16[32,2048]{1,0:T(8,128)(2,1)} %shared_down_ref) | copy-start | bytes 393220
  1.3 46.0 %copy-start.6 = (f32[2048]{0:T(1024)S(1)}, f32[2048]{0:T(1024)}, u32[]{:S(2)}) copy-start(f32[2048]{0:T(1024)} %param.33) | copy-start | bytes 24580

commit v3 on v2

--- a/solution.py
+++ b/solution.py
@@ -12,9 +12,7 @@
 EP, TA, TB = 16, 4, 4
 ROWS = 16
 SLOTS = 4
-GROUP = 4
-HEAD_ROWS = 256
-TILE = 16
+LATE = 7
 BLOCKS = 16
 MIB = 1024 * 1024
 
@@ -107,6 +105,10 @@
     key_hbm,
     value_hbm,
     wout_hbm,
+    *rest,
+):
+    late_hbm, rest = rest[:LATE], rest[LATE:]
+    (
     out_ref,
     new_keys_hbm,
     new_values_hbm,
@@ -114,6 +116,10 @@
     pick_ref,
     coef_hi_ref,
     coef_lo_ref,
+    *rest,
+    ) = rest
+    late_refs, rest = rest[:LATE], rest[LATE:]
+    (
     bias_buf,
     lengths_buf,
     norm_gain_buf,
@@ -140,7 +146,8 @@
     key_sem,
     value_sem,
     out_sem,
-):
+    late_sem,
+    ) = rest
     a, b = lax.axis_index("ta"), lax.axis_index("tb")
     small = [
         pltpu.make_async_copy(src, dst, small_sem.at[n])
@@ -168,71 +175,43 @@
             )
         )
     ]
+    late = [
+        pltpu.make_async_copy(src, dst, late_sem.at[n])
+        for n, (src, dst) in enumerate(zip(late_hbm, late_refs))
+    ]
     cache_len = key_buf.shape[1]
     head_size = key_buf.shape[2]
-    caches = ((key_hbm, key_buf, key_sem), (value_hbm, value_buf, value_sem))
-    head_copies = [
-        pltpu.make_async_copy(
-            src.at[:, pl.ds(0, HEAD_ROWS)], dst.at[:, pl.ds(0, HEAD_ROWS)], sems.at[ROWS]
-        )
-        for src, dst, sems in caches
-    ]
-    for copy in small + large[:2] + head_copies[:1]:
+    key_head = pltpu.make_async_copy(key_hbm, key_buf, key_sem.at[ROWS])
+    value_copies = [pltpu.make_async_copy(value_hbm, value_buf, value_sem.at[ROWS])]
+    for copy in small + large[:4] + [key_head] + value_copies + large[4:] + late:
         copy.start()
-    value_buf[:, HEAD_ROWS:, :] = jnp.zeros(
-        (ROWS, cache_len - HEAD_ROWS, head_size), value_buf.dtype
-    )
-    small[0].wait()
-    small[1].wait()
-
-    def tail_copy(cache, s):
-        src, dst, sems = cache
-        tiles = jnp.maximum((lengths_buf[s] + TILE - 1) // TILE, HEAD_ROWS // TILE + 1)
-        size = pl.multiple_of((tiles - HEAD_ROWS // TILE) * TILE, TILE)
-        part = pl.ds(HEAD_ROWS, size)
-        return pltpu.make_async_copy(src.at[s, part], dst.at[s, part], sems.at[s])
-
-    key_copies, value_copies = ([tail_copy(cache, s) for s in range(ROWS)] for cache in caches)
-    for copy in key_copies + head_copies[1:]:
-        copy.start()
-
-    for copy in small[2:]:
+
+    for copy in small + large[:4]:
         copy.wait()
-    route_tables(
-        routes_buf[...], route_weight_buf[...], a, pick_ref, coef_hi_ref, coef_lo_ref
-    )
     for s in range(ROWS):
         length_rows[s : s + 1, :] = jnp.full((1, LANES), lengths_buf[s], jnp.int32)
-    for copy in large[:2]:
-        copy.wait()
     normed = rms_rows(tokens_buf[...].astype(F32), norm_gain_buf[...]).astype(BF16)
     q_buf[...] = (
         rms_rows(dot(normed, wq_buf[...]), query_gain_buf[...]).astype(BF16).astype(F32)
     )
-    for j in range(TA):
-        cols = pl.ds(pl.multiple_of((j * TB + b) * LANES, LANES), LANES)
-        tok_slice_ref[j * ROWS : (j + 1) * ROWS, :] = tokens_buf[:, cols].astype(F32)
-
-    head_copies[0].wait()
-    for g in range(ROWS // GROUP):
-        members = range(g * GROUP, (g + 1) * GROUP)
-        for s in members:
-            key_copies[s].wait()
-        for s in members:
-            value_copies[s].start()
-        for s in members:
-            z_buf[s : s + 1, :] = dot_nt(q_buf[s : s + 1, :].astype(BF16), key_buf[s])
-
-    for copy in large[2:]:
-        copy.start()
-    for copy in large[2:4]:
-        copy.wait()
     new_keys_buf[...] = rms_rows(dot(normed, wk_buf[...]), key_gain_buf[...]).astype(BF16)
     new_values_buf[...] = dot(normed, wv_buf[...]).astype(BF16)
     out_copies = [
         pltpu.make_async_copy(new_keys_buf, new_keys_hbm, out_sem.at[0]),
         pltpu.make_async_copy(new_values_buf, new_values_hbm, out_sem.at[1]),
     ]
+    for copy in out_copies:
+        copy.start()
+    route_tables(
+        routes_buf[...], route_weight_buf[...], a, pick_ref, coef_hi_ref, coef_lo_ref
+    )
+    for j in range(TA):
+        cols = pl.ds(pl.multiple_of((j * TB + b) * LANES, LANES), LANES)
+        tok_slice_ref[j * ROWS : (j + 1) * ROWS, :] = tokens_buf[:, cols].astype(F32)
+
+    key_head.wait()
+    for s in range(ROWS):
+        z_buf[s : s + 1, :] = dot_nt(q_buf[s : s + 1, :].astype(BF16), key_buf[s])
 
     chunks = cache_len // LANES
     after = lax.broadcasted_iota(jnp.int32, (3 * LANES, LANES), 0) % LANES
@@ -264,16 +243,10 @@
         w_buf[:, cols] = jnp.where(visible[c], jnp.exp(log_beta[:, cols] + later_sum), 0.0)
         carry = carry + totals[c * ROWS : (c + 1) * ROWS, :]
 
-    for copy in out_copies:
-        copy.start()
-    head_copies[1].wait()
-    for g in range(ROWS // GROUP):
-        members = range(g * GROUP, (g + 1) * GROUP)
-        for s in members:
-            value_copies[s].wait()
-        for s in members:
-            att_buf[s : s + 1, :] = dot(w_buf[s : s + 1, :].astype(BF16), value_buf[s])
-    large[4].wait()
+    for copy in value_copies + large[4:]:
+        copy.wait()
+    for s in range(ROWS):
+        att_buf[s : s + 1, :] = dot(w_buf[s : s + 1, :].astype(BF16), value_buf[s])
     attn = dot(att_buf[...].astype(BF16), wout_buf[...]).astype(BF16)
     for t in range(BLOCKS):
         block = attn[:, t * LANES : (t + 1) * LANES]
@@ -281,7 +254,7 @@
         for n in range(TA):
             start = (n * TB + quarter) * 64 + j * ROWS
             out_ref[start : start + ROWS, :] = block
-    for copy in out_copies:
+    for copy in out_copies + late:
         copy.wait()
 
 
@@ -300,6 +273,7 @@
     keys,
     values,
     wout,
+    *late,
 ):
     rows, cache_len, head_size = keys.shape
     width = tokens.shape[1]
@@ -315,9 +289,10 @@
             shape((1024, 64), BF16),
             shape((rows, 1024), BF16),
             shape((rows, 1024), BF16),
+            *(shape(x.shape, x.dtype) for x in late),
         ),
-        in_specs=[hbm()] * 14,
-        out_specs=(vmem(), hbm(), hbm(), vmem(), vmem(), vmem(), vmem()),
+        in_specs=[hbm()] * (14 + LATE),
+        out_specs=(vmem(), hbm(), hbm()) + (vmem(),) * (4 + LATE),
         scratch_shapes=[
             pltpu.SMEM(bias.shape, F32),
             pltpu.SMEM(lengths.shape, jnp.int32),
@@ -345,6 +320,7 @@
             pltpu.SemaphoreType.DMA((rows + 1,)),
             pltpu.SemaphoreType.DMA((rows + 1,)),
             pltpu.SemaphoreType.DMA((2,)),
+            pltpu.SemaphoreType.DMA((LATE,)),
         ],
         cost_estimate=pl.CostEstimate(
             flops=2_000_000_000, bytes_accessed=10 * MIB, transcendentals=0
@@ -366,6 +342,7 @@
         keys,
         values,
         wout,
+        *late,
         ))
     )
 
@@ -504,7 +481,7 @@
     shared_up,
     shared_down,
 ):
-    partial_rows, new_keys, new_values, tok_slice, pick, coef_hi, coef_lo = attention(
+    partial_rows, new_keys, new_values, tok_slice, pick, coef_hi, coef_lo, *late = attention(
         score_bias[None, :],
         lengths,
         norm_gain[None, :],
@@ -519,15 +496,6 @@
         key_cache,
         value_cache,
         w_out,
-    )
-    later = (post_gain, expert_gate, expert_up, expert_down, shared_gate, shared_up, shared_down)
-    partial_rows, *later = lax.optimization_barrier((partial_rows, *later))
-    post_gain, expert_gate, expert_up, expert_down, shared_gate, shared_up, shared_down = later
-    arrived = exchange(partial_rows, ("ta", "tb"), TA * TB)
-    outgoing, own = dispatch(arrived, tok_slice, pick)
-    received = exchange(outgoing, ("ep", "tb"), EP * TB)
-    parts = run_experts(
-        received,
         post_gain[None, :],
         expert_gate[0],
         expert_up[0],
@@ -536,6 +504,10 @@
         shared_up.T,
         shared_down,
     )
+    arrived = exchange(partial_rows, ("ta", "tb"), TA * TB)
+    outgoing, own = dispatch(arrived, tok_slice, pick)
+    received = exchange(outgoing, ("ep", "tb"), EP * TB)
+    parts = run_experts(received, *late)
     returned = exchange(parts, ("ep", "ta", "tb"), EP * TA * TB)
     mixed = combine(returned, coef_hi, coef_lo, own)
     return (mixed, new_keys, new_values)

time: 71.1 us -> 70.2 us (0.987)
  Pallas kernels: 9.04 us -> 8.22 us
    pallas_call x1, Pallas kernels: 6.97 us -> 6.12 us  [attention(): pl.pallas_call(attention_kernel, name='attention', out_shape=(shape((1024...]
where the time goes in v3:
time: 70.2 us; the launch traced here: 70 us
  blocking collectives  60.5 us (86%)
  Pallas kernels  8.22 us (12%)
  between operations  1.31 us (2%)
    all_to_all x3, blocking collectives, exchange(): lax.all_to_all(pieces, axes, split_axis=0, concat_axis=0, tiled=True)  60.5 us
    pallas_call x1, Pallas kernels, attention(): pl.pallas_call(attention_kernel, name='attention', out_shape=(shape((1024...  6.12 us

profile of v3, /device:TPU:1, one launch (start us, length us, event | category | flops | bytes accessed | tf_op | source)
XLA Modules:
  0.0 70.0 jit_solution(48408615188895221)
XLA Ops:
  1.3 6.1 %attention.1 = (bf16[1024,128]{1,0:T(8,128)(2,1)S(1)}, bf16[16,128]{1,0:T(8,128)(2,1)}, bf16[16,128]{1,0:T(8,128)(2,1)}, f32[64,128]{1,0:T(8,128)S(1)}, bf16[102...) custom-call(f32[1,1]{1,0:T(1,128)} %bitcast.18.bias_hbm, ...), custom_call_target="tpu_custom_call" | custom-call | flops 2000000000 | bytes 10485760 | tf_op jit(solution)/shard_map/attention/pallas_call | solution.py:281
  7.4 21.4 %all_to_all.15 = bf16[16,64,128]{2,1,0:T(8,128)(2,1)S(1)} all-to-all(bf16[16,64,128]{2,1,0:T(8,128)(2,1)S(1)} %bitcast.19), channel_id=1, replica_groups=mesh['ep'=16,'ta'=4,'tb'=4] {'ta','tb'}, dimensions={0} | all-to-all | bytes 524288 | tf_op jit(solution)/shard_map/all_to_all | solution.py:457
  28.8 0.2 dispatch.1
  29.0 17.4 %all_to_all.16 = bf16[64,16,128]{2,1,0:T(8,128)(2,1)S(1)} all-to-all(bf16[64,16,128]{2,1,0:T(8,128)(2,1)S(1)} %bitcast.23), channel_id=1, replica_groups=mesh['ep'=16,'ta'=4,'tb'=4] {'ep','tb'}, dimensions={0} | all-to-all | bytes 524288 | tf_op jit(solution)/shard_map/all_to_all | solution.py:457
  46.4 1.1 %experts.1 = bf16[1024,128]{1,0:T(8,128)(2,1)S(1)} custom-call(bf16[1024,128]{1,0:T(8,128)(2,1)S(1)} %bitcast.20, f32[1,2048]{1,0:T(1,128)S(1)} %get-tuple-element.23.post_gain_ref, bf16[2048,128]{1,0:T(8,128)(2,1)S(1)} %get-tuple-element.24.gate_ref, bf16[2048,128]{1,0:T(8,128)(2,1)S(1)} %get-tuple-element.25.up_ref, ...), custom_call_target="tpu_custom_call" | custom-call | flops 1000000000 | bytes 3145728 | tf_op jit(solution)/shard_map/experts/pallas_call | solution.py:417
  47.5 21.7 %all_to_all.17 = bf16[256,4,128]{2,1,0:T(4,128)(2,1)S(1)} all-to-all(bf16[256,4,128]{2,1,0:T(4,128)(2,1)S(1)} %bitcast.21), channel_id=1, replica_groups=mesh['ep'=16,'ta'=4,'tb'=4] {'ep','ta','tb'}, dimensions={0} | all-to-all | bytes 524288 | tf_op jit(solution)/shard_map/all_to_all | solution.py:457
  69.2 0.8 %combine.1 = bf16[16,128]{1,0:T(8,128)(2,1)} custom-call(bf16[1024,128]{1,0:T(8,128)(2,1)S(1)} %bitcast.24, bf16[16,1024]{1,0:T(8,128)(2,1)S(1)} %get-tuple-element.30.coef_hi_ref, bf16[16,1024]{1,0:T(8,128)(2,1)S(1)} %get-tuple-element.31.coef_lo_ref, f32[16,128]{1,0:T(8,128)S(1)} %get-tuple-element.32.own_ref), custom_call_target="tpu_custom_call" | custom-call | flops 100000000 | bytes 1048576 | tf_op jit(solution)/shard_map/combine/pallas_call | solution.py:442

commit v4 on v3

--- a/solution.py
+++ b/solution.py
@@ -12,7 +12,8 @@
 EP, TA, TB = 16, 4, 4
 ROWS = 16
 SLOTS = 4
-LATE = 7
+SMALL = 6
+LATE = 10
 BLOCKS = 16
 MIB = 1024 * 1024
 
@@ -90,87 +91,29 @@
     coef_lo_ref[...] = jnp.where(is_shared | ~held, 0.0, by_col[2 * ROWS :]).astype(BF16)
 
 
-def attention_kernel(
-    bias_hbm,
-    lengths_hbm,
-    norm_gain_hbm,
-    query_gain_hbm,
-    key_gain_hbm,
-    routes_hbm,
-    route_weight_hbm,
-    tokens_hbm,
-    wq_hbm,
-    wk_hbm,
-    wv_hbm,
-    key_hbm,
-    value_hbm,
-    wout_hbm,
-    *rest,
-):
-    late_hbm, rest = rest[:LATE], rest[LATE:]
-    (
-    out_ref,
-    new_keys_hbm,
-    new_values_hbm,
-    tok_slice_ref,
-    pick_ref,
-    coef_hi_ref,
-    coef_lo_ref,
-    *rest,
-    ) = rest
-    late_refs, rest = rest[:LATE], rest[LATE:]
-    (
-    bias_buf,
-    lengths_buf,
-    norm_gain_buf,
-    query_gain_buf,
-    key_gain_buf,
-    routes_buf,
-    route_weight_buf,
-    tokens_buf,
-    wq_buf,
-    wk_buf,
-    wv_buf,
-    key_buf,
-    value_buf,
-    wout_buf,
-    q_buf,
-    z_buf,
-    w_buf,
-    att_buf,
-    length_rows,
-    new_keys_buf,
-    new_values_buf,
-    small_sem,
-    sem,
-    key_sem,
-    value_sem,
-    out_sem,
-    late_sem,
-    ) = rest
+def attention_kernel(*refs):
+    small_hbm, refs = refs[:SMALL], refs[SMALL:]
+    tokens_hbm, wq_hbm, key_hbm, value_hbm, wout_hbm, *refs = refs
+    late_hbm, refs = refs[:LATE], refs[LATE:]
+    out_ref, normed_ref, tok_slice_ref, pick_ref, coef_hi_ref, coef_lo_ref, *refs = refs
+    late_refs, refs = refs[:LATE], refs[LATE:]
+    small_bufs, refs = refs[:SMALL], refs[SMALL:]
+    tokens_buf, wq_buf, key_buf, value_buf, wout_buf, *refs = refs
+    q_buf, z_buf, w_buf, att_buf, length_rows, small_sem, sem, late_sem = refs
+    lengths_buf, bias_buf, routes_buf, route_weight_buf, norm_gain_buf, query_gain_buf = small_bufs
     a, b = lax.axis_index("ta"), lax.axis_index("tb")
     small = [
         pltpu.make_async_copy(src, dst, small_sem.at[n])
-        for n, (src, dst) in enumerate(
-            (
-                (lengths_hbm, lengths_buf),
-                (bias_hbm, bias_buf),
-                (routes_hbm, routes_buf),
-                (route_weight_hbm, route_weight_buf),
-                (norm_gain_hbm, norm_gain_buf),
-                (query_gain_hbm, query_gain_buf),
-                (key_gain_hbm, key_gain_buf),
-            )
-        )
+        for n, (src, dst) in enumerate(zip(small_hbm, small_bufs))
     ]
-    large = [
+    tokens_copy, wq_copy, key_copy, value_copy, wout_copy = large = [
         pltpu.make_async_copy(src, dst, sem.at[n])
         for n, (src, dst) in enumerate(
             (
                 (tokens_hbm, tokens_buf),
                 (wq_hbm, wq_buf),
-                (wk_hbm, wk_buf),
-                (wv_hbm, wv_buf),
+                (key_hbm, key_buf),
+                (value_hbm, value_buf),
                 (wout_hbm, wout_buf),
             )
         )
@@ -179,14 +122,12 @@
         pltpu.make_async_copy(src, dst, late_sem.at[n])
         for n, (src, dst) in enumerate(zip(late_hbm, late_refs))
     ]
+    for copy in small + large + late:
+        copy.start()
+
     cache_len = key_buf.shape[1]
     head_size = key_buf.shape[2]
-    key_head = pltpu.make_async_copy(key_hbm, key_buf, key_sem.at[ROWS])
-    value_copies = [pltpu.make_async_copy(value_hbm, value_buf, value_sem.at[ROWS])]
-    for copy in small + large[:4] + [key_head] + value_copies + large[4:] + late:
-        copy.start()
-
-    for copy in small + large[:4]:
+    for copy in small + [tokens_copy, wq_copy]:
         copy.wait()
     for s in range(ROWS):
         length_rows[s : s + 1, :] = jnp.full((1, LANES), lengths_buf[s], jnp.int32)
@@ -194,14 +135,7 @@
     q_buf[...] = (
         rms_rows(dot(normed, wq_buf[...]), query_gain_buf[...]).astype(BF16).astype(F32)
     )
-    new_keys_buf[...] = rms_rows(dot(normed, wk_buf[...]), key_gain_buf[...]).astype(BF16)
-    new_values_buf[...] = dot(normed, wv_buf[...]).astype(BF16)
-    out_copies = [
-        pltpu.make_async_copy(new_keys_buf, new_keys_hbm, out_sem.at[0]),
-        pltpu.make_async_copy(new_values_buf, new_values_hbm, out_sem.at[1]),
-    ]
-    for copy in out_copies:
-        copy.start()
+    normed_ref[...] = normed
     route_tables(
         routes_buf[...], route_weight_buf[...], a, pick_ref, coef_hi_ref, coef_lo_ref
     )
@@ -209,7 +143,7 @@
         cols = pl.ds(pl.multiple_of((j * TB + b) * LANES, LANES), LANES)
         tok_slice_ref[j * ROWS : (j + 1) * ROWS, :] = tokens_buf[:, cols].astype(F32)
 
-    key_head.wait()
+    key_copy.wait()
     for s in range(ROWS):
         z_buf[s : s + 1, :] = dot_nt(q_buf[s : s + 1, :].astype(BF16), key_buf[s])
 
@@ -243,8 +177,8 @@
         w_buf[:, cols] = jnp.where(visible[c], jnp.exp(log_beta[:, cols] + later_sum), 0.0)
         carry = carry + totals[c * ROWS : (c + 1) * ROWS, :]
 
-    for copy in value_copies + large[4:]:
-        copy.wait()
+    value_copy.wait()
+    wout_copy.wait()
     for s in range(ROWS):
         att_buf[s : s + 1, :] = dot(w_buf[s : s + 1, :].astype(BF16), value_buf[s])
     attn = dot(att_buf[...].astype(BF16), wout_buf[...]).astype(BF16)
@@ -254,56 +188,36 @@
         for n in range(TA):
             start = (n * TB + quarter) * 64 + j * ROWS
             out_ref[start : start + ROWS, :] = block
-    for copy in out_copies + late:
+    for copy in late:
         copy.wait()
 
 
-def attention(
-    bias,
-    lengths,
-    norm_gain,
-    query_gain,
-    key_gain,
-    routes,
-    route_weight,
-    tokens,
-    wq,
-    wk,
-    wv,
-    keys,
-    values,
-    wout,
-    *late,
-):
+def attention(small, tokens, wq, keys, values, wout, late):
     rows, cache_len, head_size = keys.shape
     width = tokens.shape[1]
     shape = jax.ShapeDtypeStruct
+    kept = [pltpu.with_memory_space_constraint(x, pltpu.HBM) for x in small if x.size > 1]
+    small = (kept[0], small[1], *kept[1:])
+    large = (tokens, wq, keys, values, wout, *late)
     return pl.pallas_call(
         attention_kernel,
         name="attention",
         out_shape=(
             shape((1024, LANES), BF16),
-            shape((rows, head_size), BF16),
-            shape((rows, head_size), BF16),
+            shape((rows, width), BF16),
             shape((64, LANES), F32),
             shape((1024, 64), BF16),
             shape((rows, 1024), BF16),
             shape((rows, 1024), BF16),
             *(shape(x.shape, x.dtype) for x in late),
         ),
-        in_specs=[hbm()] * (14 + LATE),
-        out_specs=(vmem(), hbm(), hbm()) + (vmem(),) * (4 + LATE),
+        in_specs=[hbm()] * (SMALL + 5 + LATE),
+        out_specs=(vmem(),) * (6 + LATE),
         scratch_shapes=[
-            pltpu.SMEM(bias.shape, F32),
-            pltpu.SMEM(lengths.shape, jnp.int32),
-            pltpu.VMEM(norm_gain.shape, F32),
-            pltpu.VMEM(query_gain.shape, F32),
-            pltpu.VMEM(key_gain.shape, F32),
-            pltpu.VMEM(routes.shape, jnp.int32),
-            pltpu.VMEM(route_weight.shape, F32),
+            pltpu.SMEM(small[0].shape, jnp.int32),
+            pltpu.SMEM(small[1].shape, F32),
+            *(pltpu.VMEM(x.shape, x.dtype) for x in small[2:]),
             pltpu.VMEM((rows, width), BF16),
-            pltpu.VMEM((width, head_size), BF16),
-            pltpu.VMEM((width, head_size), BF16),
             pltpu.VMEM((width, head_size), BF16),
             pltpu.VMEM((rows, cache_len, head_size), BF16),
             pltpu.VMEM((rows, cache_len, head_size), BF16),
@@ -313,38 +227,15 @@
             pltpu.VMEM((rows, cache_len), F32),
             pltpu.VMEM((rows, head_size), F32),
             pltpu.VMEM((rows, LANES), jnp.int32),
-            pltpu.VMEM((rows, head_size), BF16),
-            pltpu.VMEM((rows, head_size), BF16),
-            pltpu.SemaphoreType.DMA((7,)),
+            pltpu.SemaphoreType.DMA((SMALL,)),
             pltpu.SemaphoreType.DMA((5,)),
-            pltpu.SemaphoreType.DMA((rows + 1,)),
-            pltpu.SemaphoreType.DMA((rows + 1,)),
-            pltpu.SemaphoreType.DMA((2,)),
             pltpu.SemaphoreType.DMA((LATE,)),
         ],
         cost_estimate=pl.CostEstimate(
-            flops=2_000_000_000, bytes_accessed=10 * MIB, transcendentals=0
+            flops=2_000_000_000, bytes_accessed=12 * MIB, transcendentals=0
         ),
         compiler_params=pltpu.CompilerParams(vmem_limit_bytes=16 * MIB),
-    )(
-        bias,
-        *(pltpu.with_memory_space_constraint(x, pltpu.HBM) for x in (
-        lengths,
-        norm_gain,
-        query_gain,
-        key_gain,
-        routes,
-        route_weight,
-        tokens,
-        wq,
-        wk,
-        wv,
-        keys,
-        values,
-        wout,
-        *late,
-        ))
-    )
+    )(*small, *(pltpu.with_memory_space_constraint(x, pltpu.HBM) for x in large))
 
 
 def dispatch_kernel(arrived_ref, tok_slice_ref, pick_ref, out_ref, own_ref, h_buf):
@@ -376,6 +267,7 @@
 
 def expert_kernel(
     arrived_ref,
+    normed_ref,
     post_gain_ref,
     gate_ref,
     up_ref,
@@ -383,11 +275,28 @@
     shared_gate_ref,
     shared_up_ref,
     shared_down_ref,
+    wk_ref,
+    wv_ref,
+    key_gain_ref,
     out_ref,
+    new_keys_hbm,
+    new_values_hbm,
     rows_buf,
     x_buf,
     send_buf,
+    new_keys_buf,
+    new_values_buf,
+    sem,
 ):
+    normed = normed_ref[...]
+    new_keys_buf[...] = rms_rows(dot(normed, wk_ref[...]), key_gain_ref[...]).astype(BF16)
+    new_values_buf[...] = dot(normed, wv_ref[...]).astype(BF16)
+    copies = [
+        pltpu.make_async_copy(new_keys_buf, new_keys_hbm, sem.at[0]),
+        pltpu.make_async_copy(new_values_buf, new_values_hbm, sem.at[1]),
+    ]
+    for copy in copies:
+        copy.start()
     rows_buf[...] = arrived_ref[...].astype(F32)
     for t in range(BLOCKS):
         j, b = t // TB, t % TB
@@ -411,25 +320,36 @@
             part = routed[s * ROWS : (s + 1) * ROWS, cols] if s < SLOTS - 1 else shared[:, cols]
             send_buf[pl.ds(t * SLOTS + s, EP, stride=64), :] = part
     out_ref[...] = send_buf[...].astype(BF16)
-
-
-def run_experts(arrived, post_gain, gate, up, down, s_gate, s_up, s_down):
+    for copy in copies:
+        copy.wait()
+
+
+def run_experts(arrived, normed, *late):
+    shape = jax.ShapeDtypeStruct
+    rows = normed.shape[0]
     return pl.pallas_call(
         expert_kernel,
         name="experts",
-        out_shape=jax.ShapeDtypeStruct((1024, LANES), BF16),
-        in_specs=[vmem()] * 8,
-        out_specs=vmem(),
+        out_shape=(
+            shape((1024, LANES), BF16),
+            shape((rows, LANES), BF16),
+            shape((rows, LANES), BF16),
+        ),
+        in_specs=[vmem()] * (2 + LATE),
+        out_specs=(vmem(), hbm(), hbm()),
         scratch_shapes=[
             pltpu.VMEM((1024, LANES), F32),
             pltpu.VMEM((64, BLOCKS * LANES), F32),
             pltpu.VMEM((1024, LANES), F32),
+            pltpu.VMEM((rows, LANES), BF16),
+            pltpu.VMEM((rows, LANES), BF16),
+            pltpu.SemaphoreType.DMA((2,)),
         ],
         cost_estimate=pl.CostEstimate(
             flops=1_000_000_000, bytes_accessed=3 * MIB, transcendentals=0
         ),
         compiler_params=pltpu.CompilerParams(vmem_limit_bytes=12 * MIB),
-    )(arrived, post_gain, gate, up, down, s_gate, s_up, s_down)
+    )(arrived, normed, *late)
 
 
 def combine_kernel(arrived_ref, coef_hi_ref, coef_lo_ref, own_ref, out_ref):
@@ -481,21 +401,15 @@
     shared_up,
     shared_down,
 ):
-    partial_rows, new_keys, new_values, tok_slice, pick, coef_hi, coef_lo, *late = attention(
+    small = (
+        lengths,
         score_bias[None, :],
-        lengths,
+        routes.T,
+        route_weight.T,
         norm_gain[None, :],
         query_gain[None, :],
-        key_gain[None, :],
-        routes.T,
-        route_weight.T,
-        tokens,
-        w_query,
-        w_key,
-        w_value,
-        key_cache,
-        value_cache,
-        w_out,
+    )
+    late = (
         post_gain[None, :],
         expert_gate[0],
         expert_up[0],
@@ -503,11 +417,17 @@
         shared_gate.T,
         shared_up.T,
         shared_down,
+        w_key,
+        w_value,
+        key_gain[None, :],
+    )
+    partial_rows, normed, tok_slice, pick, coef_hi, coef_lo, *late = attention(
+        small, tokens, w_query, key_cache, value_cache, w_out, late
     )
     arrived = exchange(partial_rows, ("ta", "tb"), TA * TB)
     outgoing, own = dispatch(arrived, tok_slice, pick)
     received = exchange(outgoing, ("ep", "tb"), EP * TB)
-    parts = run_experts(received, *late)
+    parts, new_keys, new_values = run_experts(received, normed, *late)
     returned = exchange(parts, ("ep", "ta", "tb"), EP * TA * TB)
     mixed = combine(returned, coef_hi, coef_lo, own)
     return (mixed, new_keys, new_values)

time: 70.2 us -> 71.8 us (1.023)
  Pallas kernels: 8.22 us -> 9.87 us
    pallas_call x1, Pallas kernels: 6.12 us -> 7.45 us  [attention(): pl.pallas_call(attention_kernel, name='attention', out_shape=(shape((1024...]
where the time goes in v4:
time: 71.8 us; the launch traced here: 71.7 us
  blocking collectives  60.5 us (84%)
  Pallas kernels  9.87 us (14%)
  between operations  1.31 us (2%)
    all_to_all x3, blocking collectives, exchange(): lax.all_to_all(pieces, axes, split_axis=0, concat_axis=0, tiled=True)  60.5 us
    pallas_call x1, Pallas kernels, attention(): pl.pallas_call(attention_kernel, name='attention', out_shape=(shape((1024...  7.45 us

profile of v4, /device:TPU:1, one launch (start us, length us, event | category | flops | bytes accessed | tf_op | source)
XLA Modules:
  0.0 71.7 jit_solution(15939849747308116697)
XLA Ops:
  1.3 7.4 %attention.1 = (bf16[1024,128]{1,0:T(8,128)(2,1)S(1)}, bf16[16,2048]{1,0:T(8,128)(2,1)S(1)}, f32[64,128]{1,0:T(8,128)S(1)}, bf16[1024,64]{1,0:T(8,128)(2,1)S(1)}...) custom-call(s32[16]{0:T(128)} %refs_0_.1, ...), custom_call_target="tpu_custom_call" | custom-call | flops 2000000000 | bytes 12582912 | tf_op jit(solution)/shard_map/attention/pallas_call | solution.py:202
  8.7 21.4 %all_to_all.15 = bf16[16,64,128]{2,1,0:T(8,128)(2,1)S(1)} all-to-all(bf16[16,64,128]{2,1,0:T(8,128)(2,1)S(1)} %bitcast.19), channel_id=1, replica_groups=mesh['ep'=16,'ta'=4,'tb'=4] {'ta','tb'}, dimensions={0} | all-to-all | bytes 524288 | tf_op jit(solution)/shard_map/all_to_all | solution.py:377
  30.1 0.2 dispatch.1
  30.3 17.4 %all_to_all.16 = bf16[64,16,128]{2,1,0:T(8,128)(2,1)S(1)} all-to-all(bf16[64,16,128]{2,1,0:T(8,128)(2,1)S(1)} %bitcast.24), channel_id=1, replica_groups=mesh['ep'=16,'ta'=4,'tb'=4] {'ep','tb'}, dimensions={0} | all-to-all | bytes 524288 | tf_op jit(solution)/shard_map/all_to_all | solution.py:377
  47.7 1.4 %experts.1 = (bf16[1024,128]{1,0:T(8,128)(2,1)S(1)}, bf16[16,128]{1,0:T(8,128)(2,1)}, bf16[16,128]{1,0:T(8,128)(2,1)}) custom-call(bf16[1024,128]{1,0:T(8,128)(2,1)S(1)} %bitcast.20, bf16[16,2048]{1,0:T(8,128)(2,1)S(1)} %get-tuple-element.28.normed_ref, f32[1,2048]{1,0:T(1,128)S(1)} %get-tuple-element.29.post_gain_ref, ...), custom_call_target="tpu_custom_call" | custom-call | flops 1000000000 | bytes 3145728 | tf_op jit(solution)/shard_map/experts/pallas_call | solution.py:330
  49.1 21.8 %all_to_all.17 = bf16[256,4,128]{2,1,0:T(4,128)(2,1)S(1)} all-to-all(bf16[256,4,128]{2,1,0:T(4,128)(2,1)S(1)} %bitcast.21), channel_id=1, replica_groups=mesh['ep'=16,'ta'=4,'tb'=4] {'ep','ta','tb'}, dimensions={0} | all-to-all | bytes 524288 | tf_op jit(solution)/shard_map/all_to_all | solution.py:377
  70.9 0.8 %combine.1 = bf16[16,128]{1,0:T(8,128)(2,1)} custom-call(bf16[1024,128]{1,0:T(8,128)(2,1)S(1)} %bitcast.22, bf16[16,1024]{1,0:T(8,128)(2,1)S(1)} %get-tuple-element.40.coef_hi_ref, bf16[16,1024]{1,0:T(8,128)(2,1)S(1)} %get-tuple-element.41.coef_lo_ref, f32[16,128]{1,0:T(8,128)S(1)} %get-tuple-element.42.own_ref), custom_call_target="tpu_custom_call" | custom-call | flops 100000000 | bytes 1048576 | tf_op jit(solution)/shard_map/combine/pallas_call | solution.py:362

commit v5 on v3

--- a/solution.py
+++ b/solution.py
@@ -183,7 +183,7 @@
     head_size = key_buf.shape[2]
     key_head = pltpu.make_async_copy(key_hbm, key_buf, key_sem.at[ROWS])
     value_copies = [pltpu.make_async_copy(value_hbm, value_buf, value_sem.at[ROWS])]
-    for copy in small + large[:4] + [key_head] + value_copies + large[4:] + late:
+    for copy in small + large[:4] + [key_head] + value_copies + large[4:]:
         copy.start()
 
     for copy in small + large[:4]:
@@ -210,6 +210,8 @@
         tok_slice_ref[j * ROWS : (j + 1) * ROWS, :] = tokens_buf[:, cols].astype(F32)
 
     key_head.wait()
+    for copy in late:
+        copy.start()
     for s in range(ROWS):
         z_buf[s : s + 1, :] = dot_nt(q_buf[s : s + 1, :].astype(BF16), key_buf[s])
 

time: 70.2 us -> 69.6 us (level)
  no operation moved by 1% of the time
where the time goes in v5:
time: 69.6 us; the launch traced here: 69.4 us
  blocking collectives  60.5 us (87%)
  Pallas kernels  7.68 us (11%)
  between operations  1.31 us (2%)
    all_to_all x3, blocking collectives, exchange(): lax.all_to_all(pieces, axes, split_axis=0, concat_axis=0, tiled=True)  60.5 us
    pallas_call x1, Pallas kernels, attention(): pl.pallas_call(attention_kernel, name='attention', out_shape=(shape((1024...  5.58 us

profile of v5, /device:TPU:1, one launch (start us, length us, event | category | flops | bytes accessed | tf_op | source)
XLA Modules:
  0.0 69.4 jit_solution(13146791703881248720)
XLA Ops:
  1.3 5.6 %attention.1 = (bf16[1024,128]{1,0:T(8,128)(2,1)S(1)}, bf16[16,128]{1,0:T(8,128)(2,1)}, bf16[16,128]{1,0:T(8,128)(2,1)}, f32[64,128]{1,0:T(8,128)S(1)}, bf16[102...) custom-call(f32[1,1]{1,0:T(1,128)} %bitcast.18.bias_hbm, ...), custom_call_target="tpu_custom_call" | custom-call | flops 2000000000 | bytes 10485760 | tf_op jit(solution)/shard_map/attention/pallas_call | solution.py:283
  6.9 21.4 %all_to_all.15 = bf16[16,64,128]{2,1,0:T(8,128)(2,1)S(1)} all-to-all(bf16[16,64,128]{2,1,0:T(8,128)(2,1)S(1)} %bitcast.19), channel_id=1, replica_groups=mesh['ep'=16,'ta'=4,'tb'=4] {'ta','tb'}, dimensions={0} | all-to-all | bytes 524288 | tf_op jit(solution)/shard_map/all_to_all | solution.py:459
  28.2 0.2 dispatch.1
  28.5 17.4 %all_to_all.16 = bf16[64,16,128]{2,1,0:T(8,128)(2,1)S(1)} all-to-all(bf16[64,16,128]{2,1,0:T(8,128)(2,1)S(1)} %bitcast.23), channel_id=1, replica_groups=mesh['ep'=16,'ta'=4,'tb'=4] {'ep','tb'}, dimensions={0} | all-to-all | bytes 524288 | tf_op jit(solution)/shard_map/all_to_all | solution.py:459
  45.8 1.1 %experts.1 = bf16[1024,128]{1,0:T(8,128)(2,1)S(1)} custom-call(bf16[1024,128]{1,0:T(8,128)(2,1)S(1)} %bitcast.20, f32[1,2048]{1,0:T(1,128)S(1)} %get-tuple-element.23.post_gain_ref, bf16[2048,128]{1,0:T(8,128)(2,1)S(1)} %get-tuple-element.24.gate_ref, bf16[2048,128]{1,0:T(8,128)(2,1)S(1)} %get-tuple-element.25.up_ref, ...), custom_call_target="tpu_custom_call" | custom-call | flops 1000000000 | bytes 3145728 | tf_op jit(solution)/shard_map/experts/pallas_call | solution.py:419
  46.9 21.7 %all_to_all.17 = bf16[256,4,128]{2,1,0:T(4,128)(2,1)S(1)} all-to-all(bf16[256,4,128]{2,1,0:T(4,128)(2,1)S(1)} %bitcast.21), channel_id=1, replica_groups=mesh['ep'=16,'ta'=4,'tb'=4] {'ep','ta','tb'}, dimensions={0} | all-to-all | bytes 524288 | tf_op jit(solution)/shard_map/all_to_all | solution.py:459
  68.7 0.8 %combine.1 = bf16[16,128]{1,0:T(8,128)(2,1)} custom-call(bf16[1024,128]{1,0:T(8,128)(2,1)S(1)} %bitcast.24, bf16[16,1024]{1,0:T(8,128)(2,1)S(1)} %get-tuple-element.30.coef_hi_ref, bf16[16,1024]{1,0:T(8,128)(2,1)S(1)} %get-tuple-element.31.coef_lo_ref, f32[16,128]{1,0:T(8,128)S(1)} %get-tuple-element.32.own_ref), custom_call_target="tpu_custom_call" | custom-call | flops 100000000 | bytes 1048576 | tf_op jit(solution)/shard_map/combine/pallas_call | solution.py:444

commit v6 on v5

--- a/solution.py
+++ b/solution.py
@@ -108,46 +108,15 @@
     *rest,
 ):
     late_hbm, rest = rest[:LATE], rest[LATE:]
-    (
-    out_ref,
-    new_keys_hbm,
-    new_values_hbm,
-    tok_slice_ref,
-    pick_ref,
-    coef_hi_ref,
-    coef_lo_ref,
-    *rest,
-    ) = rest
+    (out_ref, new_keys_hbm, new_values_hbm, tok_slice_ref), rest = rest[:4], rest[4:]
+    (pick_ref, coef_hi_ref, coef_lo_ref), rest = rest[:3], rest[3:]
     late_refs, rest = rest[:LATE], rest[LATE:]
-    (
-    bias_buf,
-    lengths_buf,
-    norm_gain_buf,
-    query_gain_buf,
-    key_gain_buf,
-    routes_buf,
-    route_weight_buf,
-    tokens_buf,
-    wq_buf,
-    wk_buf,
-    wv_buf,
-    key_buf,
-    value_buf,
-    wout_buf,
-    q_buf,
-    z_buf,
-    w_buf,
-    att_buf,
-    length_rows,
-    new_keys_buf,
-    new_values_buf,
-    small_sem,
-    sem,
-    key_sem,
-    value_sem,
-    out_sem,
-    late_sem,
-    ) = rest
+    (bias_buf, lengths_buf, norm_gain_buf, query_gain_buf), rest = rest[:4], rest[4:]
+    (key_gain_buf, routes_buf, route_weight_buf, tokens_buf), rest = rest[:4], rest[4:]
+    (wq_buf, wk_buf, wv_buf, key_buf, value_buf, wout_buf), rest = rest[:6], rest[6:]
+    (q_buf, z_buf, w_buf, att_buf, length_rows), rest = rest[:5], rest[5:]
+    (new_keys_buf, new_values_buf), sems = rest[:2], rest[2:]
+    small_sem, sem, key_sem, value_sem, out_sem, late_sem = sems
     a, b = lax.axis_index("ta"), lax.axis_index("tb")
     small = [
         pltpu.make_async_copy(src, dst, small_sem.at[n])
@@ -181,9 +150,9 @@
     ]
     cache_len = key_buf.shape[1]
     head_size = key_buf.shape[2]
-    key_head = pltpu.make_async_copy(key_hbm, key_buf, key_sem.at[ROWS])
-    value_copies = [pltpu.make_async_copy(value_hbm, value_buf, value_sem.at[ROWS])]
-    for copy in small + large[:4] + [key_head] + value_copies + large[4:]:
+    key_copy = pltpu.make_async_copy(key_hbm, key_buf, key_sem.at[0])
+    value_copy = pltpu.make_async_copy(value_hbm, value_buf, value_sem.at[0])
+    for copy in small + large[:4] + [key_copy, value_copy] + large[4:]:
         copy.start()
 
     for copy in small + large[:4]:
@@ -209,7 +178,7 @@
         cols = pl.ds(pl.multiple_of((j * TB + b) * LANES, LANES), LANES)
         tok_slice_ref[j * ROWS : (j + 1) * ROWS, :] = tokens_buf[:, cols].astype(F32)
 
-    key_head.wait()
+    key_copy.wait()
     for copy in late:
         copy.start()
     for s in range(ROWS):
@@ -245,7 +214,7 @@
         w_buf[:, cols] = jnp.where(visible[c], jnp.exp(log_beta[:, cols] + later_sum), 0.0)
         carry = carry + totals[c * ROWS : (c + 1) * ROWS, :]
 
-    for copy in value_copies + large[4:]:
+    for copy in [value_copy] + large[4:]:
         copy.wait()
     for s in range(ROWS):
         att_buf[s : s + 1, :] = dot(w_buf[s : s + 1, :].astype(BF16), value_buf[s])
@@ -319,8 +288,8 @@
             pltpu.VMEM((rows, head_size), BF16),
             pltpu.SemaphoreType.DMA((7,)),
             pltpu.SemaphoreType.DMA((5,)),
-            pltpu.SemaphoreType.DMA((rows + 1,)),
-            pltpu.SemaphoreType.DMA((rows + 1,)),
+            pltpu.SemaphoreType.DMA((1,)),
+            pltpu.SemaphoreType.DMA((1,)),
             pltpu.SemaphoreType.DMA((2,)),
             pltpu.SemaphoreType.DMA((LATE,)),
         ],
@@ -330,22 +299,25 @@
         compiler_params=pltpu.CompilerParams(vmem_limit_bytes=16 * MIB),
     )(
         bias,
-        *(pltpu.with_memory_space_constraint(x, pltpu.HBM) for x in (
-        lengths,
-        norm_gain,
-        query_gain,
-        key_gain,
-        routes,
-        route_weight,
-        tokens,
-        wq,
-        wk,
-        wv,
-        keys,
-        values,
-        wout,
-        *late,
-        ))
+        *(
+            pltpu.with_memory_space_constraint(x, pltpu.HBM)
+            for x in (
+                lengths,
+                norm_gain,
+                query_gain,
+                key_gain,
+                routes,
+                route_weight,
+                tokens,
+                wq,
+                wk,
+                wv,
+                keys,
+                values,
+                wout,
+                *late,
+            )
+        ),
     )
 
 
@@ -390,7 +362,8 @@
     x_buf,
     send_buf,
 ):
-    rows_buf[...] = arrived_ref[...].astype(F32)
+    count = arrived_ref.shape[0]
+    rows_buf[:count, :] = arrived_ref[...].astype(F32)
     for t in range(BLOCKS):
         j, b = t // TB, t % TB
         for s in range(SLOTS):
@@ -412,7 +385,7 @@
         for s in range(SLOTS):
             part = routed[s * ROWS : (s + 1) * ROWS, cols] if s < SLOTS - 1 else shared[:, cols]
             send_buf[pl.ds(t * SLOTS + s, EP, stride=64), :] = part
-    out_ref[...] = send_buf[...].astype(BF16)
+    out_ref[...] = send_buf[:count, :].astype(BF16)
 
 
 def run_experts(arrived, post_gain, gate, up, down, s_gate, s_up, s_down):
@@ -423,9 +396,9 @@
         in_specs=[vmem()] * 8,
         out_specs=vmem(),
         scratch_shapes=[
-            pltpu.VMEM((1024, LANES), F32),
+            pltpu.VMEM((1024 + 64, LANES), F32),
             pltpu.VMEM((64, BLOCKS * LANES), F32),
-            pltpu.VMEM((1024, LANES), F32),
+            pltpu.VMEM((1024 + 64, LANES), F32),
         ],
         cost_estimate=pl.CostEstimate(
             flops=1_000_000_000, bytes_accessed=3 * MIB, transcendentals=0

time: 69.6 us -> 69.3 us (level)
  no operation moved by 1% of the time
where the time goes in v6:
time: 69.3 us; the launch traced here: 69.2 us
  blocking collectives  60.5 us (87%)
  Pallas kernels  7.39 us (11%)
  between operations  1.31 us (2%)
    all_to_all x3, blocking collectives, exchange(): lax.all_to_all(pieces, axes, split_axis=0, concat_axis=0, tiled=True)  60.5 us
    pallas_call x1, Pallas kernels, attention(): pl.pallas_call(attention_kernel, name='attention', out_shape=(shape((1024...  5.3 us

profile of v6, /device:TPU:1, one launch (start us, length us, event | category | flops | bytes accessed | tf_op | source)
XLA Modules:
  0.0 69.2 jit_solution(6967494087185662486)
XLA Ops:
  1.3 5.3 %attention.1 = (bf16[1024,128]{1,0:T(8,128)(2,1)S(1)}, bf16[16,128]{1,0:T(8,128)(2,1)}, bf16[16,128]{1,0:T(8,128)(2,1)}, f32[64,128]{1,0:T(8,128)S(1)}, bf16[102...) custom-call(f32[1,1]{1,0:T(1,128)} %bitcast.18.bias_hbm, ...), custom_call_target="tpu_custom_call" | custom-call | flops 2000000000 | bytes 10485760 | tf_op jit(solution)/shard_map/attention/pallas_call | solution.py:252
  6.6 21.4 %all_to_all.15 = bf16[16,64,128]{2,1,0:T(8,128)(2,1)S(1)} all-to-all(bf16[16,64,128]{2,1,0:T(8,128)(2,1)S(1)} %bitcast.19), channel_id=1, replica_groups=mesh['ep'=16,'ta'=4,'tb'=4] {'ta','tb'}, dimensions={0} | all-to-all | bytes 524288 | tf_op jit(solution)/shard_map/all_to_all | solution.py:432
  27.9 0.2 dispatch.1
  28.2 17.4 %all_to_all.16 = bf16[64,16,128]{2,1,0:T(8,128)(2,1)S(1)} all-to-all(bf16[64,16,128]{2,1,0:T(8,128)(2,1)S(1)} %bitcast.23), channel_id=1, replica_groups=mesh['ep'=16,'ta'=4,'tb'=4] {'ep','tb'}, dimensions={0} | all-to-all | bytes 524288 | tf_op jit(solution)/shard_map/all_to_all | solution.py:432
  45.5 1.1 %experts.1 = bf16[1024,128]{1,0:T(8,128)(2,1)S(1)} custom-call(bf16[1024,128]{1,0:T(8,128)(2,1)S(1)} %bitcast.20, f32[1,2048]{1,0:T(1,128)S(1)} %get-tuple-element.23.post_gain_ref, bf16[2048,128]{1,0:T(8,128)(2,1)S(1)} %get-tuple-element.24.gate_ref, bf16[2048,128]{1,0:T(8,128)(2,1)S(1)} %get-tuple-element.25.up_ref, ...), custom_call_target="tpu_custom_call" | custom-call | flops 1000000000 | bytes 3145728 | tf_op jit(solution)/shard_map/experts/pallas_call | solution.py:392
  46.6 21.7 %all_to_all.17 = bf16[256,4,128]{2,1,0:T(4,128)(2,1)S(1)} all-to-all(bf16[256,4,128]{2,1,0:T(4,128)(2,1)S(1)} %bitcast.21), channel_id=1, replica_groups=mesh['ep'=16,'ta'=4,'tb'=4] {'ep','ta','tb'}, dimensions={0} | all-to-all | bytes 524288 | tf_op jit(solution)/shard_map/all_to_all | solution.py:432
  68.4 0.8 %combine.1 = bf16[16,128]{1,0:T(8,128)(2,1)} custom-call(bf16[1024,128]{1,0:T(8,128)(2,1)S(1)} %bitcast.24, bf16[16,1024]{1,0:T(8,128)(2,1)S(1)} %get-tuple-element.30.coef_hi_ref, bf16[16,1024]{1,0:T(8,128)(2,1)S(1)} %get-tuple-element.31.coef_lo_ref, f32[16,128]{1,0:T(8,128)S(1)} %get-tuple-element.32.own_ref), custom_call_target="tpu_custom_call" | custom-call | flops 100000000 | bytes 1048576 | tf_op jit(solution)/shard_map/combine/pallas_call | solution.py:417
